TPU v7x, 128 devices: a whole 4x4x4 slice. The times are simulated.
128 devices in a mesh: sp: 32 (over z, y, core), tp: 4 (over x).
Axes of the slice: x: 4, y: 4, z: 4, core: 2. Of those that a mesh axis runs over, the one named last changes fastest.
Arguments:
- tokens: bfloat16 [4096, 6, 2048], P(('sp', 'tp')), may hold values from -6 to 6
- norm_gain: float32 [2048], replicated, may hold values from 0.1 to 1.9
- w_query: bfloat16 [3, 2048, 1024], P(None, 'sp', 'tp'), may hold values from -0.125 to 0.125
- w_key: bfloat16 [3, 2048, 1024], P(None, 'sp', 'tp'), may hold values from -0.125 to 0.125
- w_value: bfloat16 [3, 2048, 1024], P(None, 'sp', 'tp'), may hold values from -0.125 to 0.125
- w_out: bfloat16 [1024, 2048], P('tp', 'sp'), may hold values from -0.1875 to 0.1875
Outputs:
- mixed: bfloat16 [4096, 6, 2048], P(('sp', 'tp'))
- log_weight: float32 [4096, 6, 8], P('sp', None, 'tp')
All inputs are finite; a program needn't handle non-finite values.
Results may differ from a plain program's by a relative error of at most 0.015.
Values may be sent and summed in bfloat16 or wider, within the bound.
A program may use at most 128 MiB of HBM per device.

v0:
```python
import math

import jax
import jax.numpy as jnp
from jax import lax
from jax.sharding import PartitionSpec as P

GROUPS = 3
HEADS = 8
STEPS = 24
DILATION_MIDDLE = 4
DILATION_WIDE = 16


epsilon = 1e-06


def from_behind(block, axis, distance):
    devices = range(lax.axis_size(axis))
    route = [(i - distance, i) for i in devices if i - distance in devices]
    return lax.ppermute(block, axis, route)


def laid_out(tiles, dim):
    shape = list(tiles.shape[1:])
    shape[dim] *= tiles.shape[0]
    return jnp.moveaxis(tiles, 0, dim).reshape(shape)


def one_gather(arrays, axis, dims):
    vector = jnp.concatenate([a.reshape(-1) for a in arrays])
    lines, at, gathered = lax.all_gather(vector, axis), 0, []
    for a, dim in zip(arrays, dims):
        tiles = lines[:, at : at + a.size].reshape(-1, *a.shape)
        gathered.append(laid_out(tiles, dim))
        at += a.size
    return tuple(gathered)


def gathered_then(shard, axis, dim, work):
    return work(lax.all_gather(shard, axis, axis=dim, tiled=True), jnp.int32(0))


def scattered(portion, width, axis):
    count = width * lax.axis_size(axis)
    sent = portion(jnp.int32(0), count).astype(jnp.bfloat16)
    return lax.psum_scatter(sent, axis, scatter_dimension=0, tiled=True).astype(jnp.float32)


def rms_normed(values, gain):
    widened = values.astype(jnp.float32)
    scaled = widened * lax.rsqrt(jnp.mean(widened * widened, axis=-1, keepdims=True) + epsilon)
    return (scaled * gain.astype(jnp.float32)).astype(jnp.bfloat16)


def reach_back(pairs, reaches):
    local_rows = pairs.shape[0]
    holding = pairs
    covered = 1
    while covered < max(reaches) + 1:
        arrived = from_behind(holding, "sp", covered)
        holding = jnp.concatenate((arrived, holding), 0)
        covered = covered * 2
    held_rows = holding.shape[0]
    extended = [
        holding[held_rows - (reach + 1) * local_rows :, :, :, group_index]
        for group_index, reach in enumerate(reaches)
    ]
    return extended


def attend_group(queries, extended, reach, dilation):
    local_rows, batch_count, local_heads, head_width = queries.shape
    span_rows = extended.shape[0]
    keys = extended[:, :, 0].reshape(
        span_rows // dilation, dilation, batch_count, local_heads, head_width
    )
    values = extended[:, :, 1].reshape(
        span_rows // dilation, dilation, batch_count, local_heads, head_width
    )
    strided = queries.reshape(
        local_rows // dilation, dilation, batch_count, local_heads, head_width
    )
    scores = jnp.einsum("qrbhe,krbhe->rbhqk", strided, keys, preferred_element_type=jnp.float32)
    scores = scores * (1.0 / math.sqrt(head_width))
    shape_steps = (local_rows // dilation, span_rows // dilation)
    query_step = lax.broadcasted_iota(jnp.int32, shape_steps, 0)
    key_step = lax.broadcasted_iota(jnp.int32, shape_steps, 1)
    lag_steps = query_step + reach * (local_rows // dilation) - key_step
    anchor = (lax.axis_index("sp") - reach) * (local_rows // dilation)
    allowed = (lag_steps >= 0) & (lag_steps <= STEPS) & (key_step + anchor >= 0)
    scores = jnp.where(allowed, scores, jnp.float32(-1e30))
    peak = jnp.max(scores, axis=-1, keepdims=True)
    lifted = jnp.exp(scores - peak)
    totals = jnp.sum(lifted, axis=-1, keepdims=True)
    log_sum = (peak + jnp.log(totals))[..., 0]
    weights = (lifted / totals).astype(jnp.bfloat16)
    mixed = jnp.einsum(
        "rbhqk,krbhe->qrbhe", weights, values, preferred_element_type=jnp.float32
    ).astype(jnp.bfloat16)
    mixed = mixed.reshape(local_rows, batch_count, local_heads, head_width)
    log_rows = jnp.transpose(log_sum, (3, 0, 1, 2)).reshape(local_rows, batch_count, local_heads)
    return (mixed, log_rows)


def shards(tokens, norm_gain, w_query, w_key, w_value, w_out):
    query_full, key_full, value_full, out_full = one_gather(
        (w_query, w_key, w_value, w_out), "sp", (1, 1, 1, 1)
    )
    roles = jnp.stack((query_full, key_full, value_full))
    normed = rms_normed(tokens, norm_gain)

    def project(piece, start):
        return jnp.einsum(
            "tbd,rgdc->tbrgc", piece, roles, preferred_element_type=jnp.float32
        ).astype(jnp.bfloat16)

    projected = gathered_then(normed, "tp", 0, project)
    local_rows = projected.shape[0]
    batch_count = projected.shape[1]
    local_heads = HEADS // lax.axis_size("tp")
    head_width = projected.shape[-1] // local_heads
    dilations = (1, DILATION_MIDDLE, DILATION_WIDE)
    reaches = tuple((-(-STEPS * dilation // local_rows) for dilation in dilations))
    pairs = projected[:, :, 1:]
    extended = [
        reach_back(pairs[:, :, :, group_index : group_index + 1], (reaches[group_index],))[0]
        for group_index in range(GROUPS)
    ]
    results = []
    for group_index in range(GROUPS):
        queries = projected[:, :, 0, group_index].reshape(
            local_rows, batch_count, local_heads, head_width
        )
        results.append(
            attend_group(
                queries, extended[group_index], reaches[group_index], dilations[group_index]
            )
        )
    stacked_logs = jnp.stack([result[1] for result in results])
    top_log = jnp.max(stacked_logs, axis=0)
    log_weight = top_log + jnp.log(jnp.sum(jnp.exp(stacked_logs - top_log[None]), axis=0))
    shares = jax.nn.softmax(stacked_logs, axis=0)
    outputs = jnp.stack([result[0] for result in results]).astype(jnp.float32)
    combined = jnp.sum(shares[..., None] * outputs, axis=0).astype(jnp.bfloat16)
    combined = combined.reshape(local_rows, batch_count, local_heads * head_width)

    def output_rows(begin, count):
        selected = lax.dynamic_slice_in_dim(combined, begin, count, 0)
        return jnp.einsum("tbc,cd->tbd", selected, out_full, preferred_element_type=jnp.float32)

    mixed = scattered(output_rows, local_rows // lax.axis_size("tp"), "tp").astype(jnp.bfloat16)
    return (mixed, log_weight)


def solution(mesh):
    in_specs = (
        P(("sp", "tp"), None, None),
        P(),
        P(None, "sp", "tp"),
        P(None, "sp", "tp"),
        P(None, "sp", "tp"),
        P("tp", "sp"),
    )
    out_specs = (P(("sp", "tp"), None, None), P("sp", None, "tp"))
    return jax.shard_map(shards, mesh=mesh, in_specs=in_specs, out_specs=out_specs, check_vma=False)
```

profile of v0, /device:TPU:0, one launch (start us, length us, event | category | flops | bytes accessed | tf_op | source)
XLA Modules:
  0.0 260.8 jit_solution(15184111302109803519)
XLA Ops:
  7.2 0.9 copy.46
  8.3 1.0 copy.75
  9.2 1.0 copy.76
  10.2 1.0 copy.77
  12.0 1.4 fusion.9
  13.4 1.1 fusion.11
  15.3 56.9 %all-gather.6.cloned.1.call-done = bf16[5242880]{0:T(1024)(128)(2,1)} async-done(((bf16[163840]{0:T(1024)(128)(2,1)}), bf16[5242880]{0:T(1024)(128)(2,1)}) %all-gather.6.cloned.1.call-update) | async-done | bytes 10485776 | tf_op jit(solution)/shard_map/all_gather | solution.py:32
  72.2 10.2 %reshape.177 = bf16[32,163840]{1,0:T(8,128)(2,1)} reshape(bf16[5242880]{0:T(1024)(128)(2,1)} %all-gather.6.cloned.1.call-done) | data formatting | bytes 20971520 | tf_op jit(solution)/shard_map/all_gather | solution.py:32
  82.4 4.1 %fusion.62 = (bf16[32,49152]{1,0:T(8,128)(2,1)S(1)}, bf16[32,49152]{1,0:T(8,128)(2,1)S(1)}, bf16[32,49152]{1,0:T(8,128)(2,1)S(1)}) fusion(bf16[32,163840]{1,0:T(8,128)(2,1)} %reshape.177), kind=kLoop, calls=%fused_computation.88 | loop fusion | bytes 18874368 | tf_op jit(solution)/shard_map/slice | solution.py:34
  86.5 0.7 copy.78
  88.3 2.2 copy.49
  91.2 2.0 copy.48
  93.3 20.0 %all-gather.4.cloned.1.call-done = bf16[128,6,2048]{2,0,1:T(8,128)(2,1)} async-done(((bf16[32,6,2048]{2,0,1:T(8,128)(2,1)}), bf16[128,6,2048]{2,0,1:T(8,128)(2,1)}) %all-gather.4.cloned.1.call-update) | async-done | bytes 3145744 | tf_op jit(solution)/shard_map/all_gather | solution.py:41
  113.3 11.4 %fusion.6 = bf16[128,6,3,3,256]{4,0,3,2,1:T(8,128)(2,1)S(1)} fusion(bf16[1,3,2048,256]{3,2,1,0:T(8,128)(2,1)} %bitcast.135, bf16[1,3,2048,256]{3,2,1,0:T(8,128)(2,1)} %bitcast.136, bf16[1,3,2048,256]{3,2,1,0:T(8,128)(2,1)S(1)} %bitcast.134, bf16[128,6,2048]{2,0,1:T(8,128)(2,1)} %all-gather.4.cloned.1.call-done), kind=kOutput, calls=%fused_computation.9 | convolution fusion | flops 7277838336 | bytes 16121856 | tf_op jit(solution)/shard_map/tbd,rgdc->tbrgc/dot_general | solution.py:114
  124.7 1.5 fusion.64
  126.1 1.1 copy-done.2
  127.3 2.4 collective-permute-start.1
  130.4 2.3 reshape.175
  132.7 1.6 copy.67
  134.3 1.4 fusion.63
  135.8 0.8 reshape.172
  136.6 0.8 reshape_reshape_squeeze.8
  137.5 3.9 %collective-permute-start = (bf16[128,6,2,1,256]{4,0,3,2,1:T(8,128)(2,1)S(1)}, bf16[128,6,2,1,256]{4,0,3,2,1:T(8,128)(2,1)}, u32[]{:S(2)}, u32[]{:S(2)}) collective-permute-start(bf16[128,6,2,1,256]{4,0,3,2,1:T(8,128)(2,1)S(1)} %copy-done.4), channel_id=1, source_target_pairs={{0,4},{4,8},{8,12},{12,16},{16,20},{20,24},{24,28},{28,32},{32,36}... | collective-permute-start | bytes 2359304 | tf_op jit(solution)/shard_map/ppermute | solution.py:21
  141.5 1.5 collective-permute-start.2
  143.0 1.5 maximum_bitcast_fusion.6
  144.5 1.0 fusion.67
  145.5 2.7 %reshape_squeeze.14 = bf16[64,4,6,2,128]{4,3,1,0,2:T(2,128)(2,1)} reshape(bf16[256,6,1,256]{3,0,2,1:T(8,128)(2,1)} %get-tuple-element.17) | data formatting | bytes 1572864 | tf_op jit(solution)/shard_map/reshape;squeeze | solution.py:75
  148.2 1.8 fusion.69
  152.5 1.3 pad_maximum_fusion
  153.8 10.8 %collective-permute-start.3 = (bf16[256,6,2,1,256]{4,0,3,2,1:T(8,128)(2,1)}, bf16[256,6,2,1,256]{4,0,3,2,1:T(8,128)(2,1)}, u32[]{:S(2)}, u32[]{:S(2)}) collective-permute-start(bf16[256,6,2,1,256]{4,0,3,2,1:T(8,128)(2,1)} %pad_maximum_fusion), channel_id=1, source_target_pairs={{0,8},{4,12},{8,16},{12,20},{16,24},{20,28},{24,32},{28,36},{32,40... | collective-permute-start | bytes 4718600 | tf_op jit(solution)/shard_map/ppermute | solution.py:21
  164.6 1.2 maximum_bitcast_fusion.5
  165.9 1.0 fusion.66
  166.9 2.7 %reshape.173 = bf16[256,6,2,128]{3,2,0,1:T(2,128)(2,1)} reshape(bf16[256,6,1,256]{3,0,2,1:T(8,128)(2,1)} %get-tuple-element.15) | data formatting | bytes 1572864 | tf_op jit(solution)/shard_map/reshape.1
  169.6 1.2 copy.73
  171.0 1.8 fusion.31
  173.3 1.6 fusion.70
  176.1 1.5 fusion.30
  177.6 19.0 %collective-permute-done.3 = bf16[256,6,2,1,256]{4,0,3,2,1:T(8,128)(2,1)} collective-permute-done((bf16[256,6,2,1,256]{4,0,3,2,1:T(8,128)(2,1)}, bf16[256,6,2,1,256]{4,0,3,2,1:T(8,128)(2,1)}, u32[]{:S(2)}, u32[]{:S(2)}) %collective-permute-start.3) | collective-permute-done | bytes 1572896 | tf_op jit(solution)/shard_map/ppermute | solution.py:21
  196.6 1.5 maximum_bitcast_fusion.2
  198.1 1.4 fusion.65
  199.5 2.4 reshape_squeeze.15
  201.8 2.1 fusion.68
  204.0 0.9 copy-done.5
  205.9 1.9 reshape_squeeze.17
  207.8 2.3 fusion.27
  210.6 1.3 multiply_reduce_fusion
  211.9 2.7 %convolution_convert_fusion = bf16[128,6,2048]{2,0,1:T(8,128)(2,1)} fusion(bf16[128,6,256]{0,2,1:T(8,128)(2,1)S(1)} %bitcast.137, bf16[256,2048,1]{0,1,2:T(8,128)(2,1)S(1)} %bitcast.133), kind=kOutput, calls=%fused_computation.6 | convolution fusion | flops 806879232 | bytes 4587520 | tf_op jit(solution)/shard_map/tbc,cd->tbd/dot_general | solution.py:150
  215.2 39.0 %reduce-scatter.2.cloned.1.call-done = bf16[32,6,2048]{2,0,1:T(8,128)(2,1)} async-done(((bf16[128,6,2048]{2,0,1:T(8,128)(2,1)}), bf16[32,6,2048]{2,0,1:T(8,128)(2,1)}) %reduce-scatter.2.cloned.1.call-update) | async-done | bytes 786448 | tf_op jit(solution)/shard_map/reduce_scatter | solution.py:47
  (82 shorter events, 10.8 us)
Async XLA Ops:
  7.2 6.2 %copy-start.3 = (bf16[32,6,2048]{2,0,1:T(8,128)(2,1)S(1)}, bf16[32,6,2048]{2,0,1:T(8,128)(2,1)}, u32[]{:S(2)}) copy-start(bf16[32,6,2048]{2,0,1:T(8,128)(2,1)} %param.6) | copy-start | bytes 2359300
  7.2 6.2 %copy-start.17 = (f32[2048]{0:T(1024)S(1)}, f32[2048]{0:T(1024)}, u32[]{:S(2)}) copy-start(f32[2048]{0:T(1024)} %param.7) | copy-start | bytes 24580
  7.2 65.0 %all-gather.6.cloned.1.call-start = ((), (), s32[]{:S(2)}) async-start(), calls=%async_computation.3 | async-start | bytes 10813440 | tf_op jit(solution)/shard_map/all_gather | solution.py:32
  12.0 101.3 %all-gather.4.cloned.1.call-start = ((), (), s32[]{:S(2)}) async-start(), calls=%async_computation.1 | async-start | bytes 3932160 | tf_op jit(solution)/shard_map/all_gather | solution.py:41
  14.6 239.7 %reduce-scatter.2.cloned.1.call-start = ((), (), s32[]{:S(2)}) async-start(), calls=%async_computation.2 | async-start | bytes 3932160 | tf_op jit(solution)/shard_map/reduce_scatter | solution.py:47
  124.7 2.6 %copy-start.2 = (bf16[128,6,3,3,256]{4,0,3,2,1:T(8,128)(2,1)}, bf16[128,6,3,3,256]{4,0,3,2,1:T(8,128)(2,1)S(1)}, u32[]{:S(2)}) copy-start(bf16[128,6,3,3,256]{4,0,3,2,1:T(8,128)(2,1)S(1)} %fusion.6) | copy-start | bytes 10616836
  124.7 5.8 %slice-start = ((bf16[32,163840]{1,0:T(8,128)(2,1)}), bf16[32,16384]{1,0:T(8,128)(2,1)S(1)}, s32[]{:S(2)}) async-start(bf16[32,163840]{1,0:T(8,128)(2,1)} %reshape.177), calls=%async_computation.4 | async-start | bytes 2097152 | tf_op jit(solution)/shard_map/slice | solution.py:34
  127.3 15.7 %collective-permute-start.1 = (bf16[128,6,2,1,256]{4,0,3,2,1:T(8,128)(2,1)}, bf16[128,6,2,1,256]{4,0,3,2,1:T(8,128)(2,1)}, u32[]{:S(2)}, u32[]{:S(2)}) collective-permute-start(bf16[128,6,2,1,256]{4,0,3,2,1:T(8,128)(2,1)} %get-tuple-element.12), channel_id=1, source_target_pairs={{0,4},{4,8},{8,12},{12,16},{16,20},{20,24},{24,28},{28,32},{32,36}... | collective-permute-start | bytes 2359304 | tf_op jit(solution)/shard_map/ppermute | solution.py:21
  134.3 3.2 %copy-start.4 = (bf16[128,6,2,1,256]{4,0,3,2,1:T(8,128)(2,1)S(1)}, bf16[128,6,2,1,256]{4,0,3,2,1:T(8,128)(2,1)}, u32[]{:S(2)}) copy-start(bf16[128,6,2,1,256]{4,0,3,2,1:T(8,128)(2,1)} %get-tuple-element.10) | copy-start | bytes 2359300
  134.3 7.1 %copy-start = (bf16[128,6,2,1,256]{4,0,3,2,1:T(8,128)(2,1)S(1)}, bf16[128,6,2,1,256]{4,0,3,2,1:T(8,128)(2,1)}, u32[]{:S(2)}) copy-start(bf16[128,6,2,1,256]{4,0,3,2,1:T(8,128)(2,1)} %get-tuple-element.11) | copy-start | bytes 2359300
  137.5 27.1 %collective-permute-start = (bf16[128,6,2,1,256]{4,0,3,2,1:T(8,128)(2,1)S(1)}, bf16[128,6,2,1,256]{4,0,3,2,1:T(8,128)(2,1)}, u32[]{:S(2)}, u32[]{:S(2)}) collective-permute-start(bf16[128,6,2,1,256]{4,0,3,2,1:T(8,128)(2,1)S(1)} %copy-done.4), channel_id=1, source_target_pairs={{0,4},{4,8},{8,12},{12,16},{16,20},{20,24},{24,28},{28,32},{32,36}... | collective-permute-start | bytes 2359304 | tf_op jit(solution)/shard_map/ppermute | solution.py:21
  141.5 11.0 %collective-permute-start.2 = (bf16[128,6,2,1,256]{4,0,3,2,1:T(8,128)(2,1)S(1)}, bf16[128,6,2,1,256]{4,0,3,2,1:T(8,128)(2,1)S(1)}, u32[]{:S(2)}, u32[]{:S(2)}) collective-permute-start(bf16[128,6,2,1,256]{4,0,3,2,1:T(8,128)(2,1)S(1)} %copy-done), channel_id=1, source_target_pairs={{0,4},{4,8},{8,12},{12,16},{16,20},{20,24},{24,28},{28,32},{32,36}... | collective-permute-start | bytes 2359304 | tf_op jit(solution)/shard_map/ppermute | solution.py:21
  150.0 0.9 copy-start.9
  150.0 0.9 copy-start.12
  153.8 42.8 %collective-permute-start.3 = (bf16[256,6,2,1,256]{4,0,3,2,1:T(8,128)(2,1)}, bf16[256,6,2,1,256]{4,0,3,2,1:T(8,128)(2,1)}, u32[]{:S(2)}, u32[]{:S(2)}) collective-permute-start(bf16[256,6,2,1,256]{4,0,3,2,1:T(8,128)(2,1)} %pad_maximum_fusion), channel_id=1, source_target_pairs={{0,8},{4,12},{8,16},{12,20},{16,24},{20,28},{24,32},{28,36},{32,40... | collective-permute-start | bytes 4718600 | tf_op jit(solution)/shard_map/ppermute | solution.py:21
  166.9 4.1 %copy-start.13 = (f32[4,6,2,32]{3,2,1,0:T(2,128)S(1)}, f32[4,6,2,32]{3,2,1,0:T(2,128)}, u32[]{:S(2)}) copy-start(f32[4,6,2,32]{3,2,1,0:T(2,128)} %copy-done.12) | copy-start | bytes 18436
  171.0 2.4 copy-start.11
  173.3 2.7 %copy-start.10 = (bf16[256,6,1,256]{0,3,1,2:T(8,128)(2,1)S(1)}, bf16[256,6,1,256]{0,3,1,2:T(8,128)(2,1)}, u32[]{:S(2)}) copy-start(bf16[256,6,1,256]{0,3,1,2:T(8,128)(2,1)} %copy.73) | copy-start | bytes 2359300
  204.0 0.9 copy-start.5
  204.0 1.5 copy-start.7
  205.5 2.3 copy-start.6
  205.6 2.2 copy-start.8
  207.8 2.8 %copy-start.15 = (f32[128,6,2]{0,2,1:T(2,128)S(1)}, f32[128,6,2]{0,2,1:T(2,128)}, u32[]{:S(2)}) copy-start(f32[128,6,2]{0,2,1:T(2,128)} %reduce_max.61) | copy-start | bytes 18436
  207.8 2.8 %copy-start.14 = (f32[1,128,6,2]{1,3,2,0:T(2,128)S(1)}, f32[1,128,6,2]{1,3,2,0:T(2,128)}, u32[]{:S(2)}) copy-start(f32[1,128,6,2]{1,3,2,0:T(2,128)} %stack.17) | copy-start | bytes 18436
  207.8 2.8 %copy-start.16 = (f32[1,128,6,2]{1,3,2,0:T(2,128)S(1)}, f32[1,128,6,2]{1,3,2,0:T(2,128)}, u32[]{:S(2)}) copy-start(f32[1,128,6,2]{1,3,2,0:T(2,128)} %fusion.58) | copy-start | bytes 18436
  210.1 1.8 copy-start.1
Sparse Core Ops, SparseCore 0:
  12.1 60.0 all-gather.5
  74.4 38.8 all-gather.3
  214.7 39.4 reduce-scatter.1
where the time goes:
time: 262 us; the launch traced here: 261 us
  waiting for transfers between devices  135 us (52%)
  local copies, waits for them, and re-layouts  53.1 us (20%)
  matrix products  25.2 us (10%)
  starting transfers between devices  18.8 us (7%)
  other arithmetic  14.5 us (6%)
  between operations  14.2 us (5%)
    all_gather x1, waiting for transfers between devices, one_gather(): lines, at, gathered = (lax.all_gather(vector, axis), 0, [])  56.9 us
    reduce_scatter x1, waiting for transfers between devices, scattered(): lax.psum_scatter(sent, axis, scatter_dimension=0, tiled=True)  39 us
    all_gather x1, waiting for transfers between devices, gathered_then(): return work(lax.all_gather(shard, axis, axis=dim, tiled=True), jnp.int32(0))  20 us
    ppermute x4, waiting for transfers between devices, from_behind(): return lax.ppermute(block, axis, route)  19 us
    ppermute x4, starting transfers between devices, from_behind(): return lax.ppermute(block, axis, route)  18.7 us
    dot_general x1, matrix products, project(): jnp.einsum('tbd,rgdc->tbrgc', piece, roles, preferred_element_type=jnp.fl...  11.4 us
    all_gather x1, local copies, waits for them, and re-layouts, one_gather(): lines, at, gathered = (lax.all_gather(vector, axis), 0, [])  10.2 us
    unnamed x43, local copies, waits for them, and re-layouts  8.43 us
  transfers between devices with their start and end apart: 7, of which 4 were waited for; matrix products, arithmetic and copies ran while one was open for 21% of the time, Pallas kernels for 0%

commit v1 on v0

v1 whole, which is shorter than its diff:
```python
import functools
import math

import jax
import jax.numpy as jnp
from jax import lax
from jax.experimental import pallas as pl
from jax.experimental.pallas import tpu as pltpu
from jax.sharding import PartitionSpec as P

MESH = pl.DeviceIdType.MESH
BATCH = 6
WIDTH = 2048
HEAD = 128
STEPS = 24
EPSILON = 1e-06
ROWS = 256
PIECE = 32
HALO = (32, 96, 384)
SPAN = (160, 224, 512)
DILATION = (1, 4, 16)
COPIES = 160
F32 = jnp.float32
BF16 = jnp.bfloat16
NT = (((1,), (1,)), ((), ()))
TN = (((0,), (0,)), ((), ()))


class Sender:
    def __init__(self, send_sem, recv_sem):
        self.send_sem, self.recv_sem, self.started = send_sem, recv_sem, []

    def __call__(self, src, dst, device):
        slot = len(self.started)
        copy = pltpu.make_async_remote_copy(
            src_ref=src,
            dst_ref=dst,
            send_sem=self.send_sem.at[slot],
            recv_sem=self.recv_sem.at[slot],
            device_id=device,
            device_id_type=MESH,
        )
        copy.start()
        self.started.append(copy)
        return copy


class PlaneGather:
    def __init__(self, send, block, a, b, to_a, to_b):
        self.send, self.block, self.a, self.b = send, block, a, b
        self.to_a, self.to_b = to_a, to_b
        self.across = {}

    def put(self, da, db, device, half=None):
        ref = self.block((self.a + da + 4) % 4, (self.b + db + 4) % 4, half)
        return self.send(ref, ref, device)

    def spread(self, da):
        for side in (1, -1):
            self.across[da, side] = self.put(da, 0, self.to_b[side])

    def begin(self):
        self.along = {side: self.put(0, 0, self.to_a[side]) for side in (1, -1)}
        self.spread(0)

    def first(self):
        self.far = {}
        for side, half in ((1, 0), (-1, 1)):
            self.along[side].wait_recv()
            self.far[side] = self.put(-side, 0, self.to_a[side], half)
            self.spread(-side)

    def second(self):
        for side in (1, -1):
            self.far[side].wait_recv()
        self.spread(2)

    def third(self):
        self.last = []
        for da, side in ((0, 1), (-1, -1), (1, 1), (2, -1)):
            self.across[da, side].wait_recv()
            self.last.append(self.put(da, -side, self.to_b[side]))

    def finish(self):
        for da, side in ((0, -1), (-1, 1), (1, -1), (2, 1)):
            self.across[da, side].wait_recv()
        for copy in self.last:
            copy.wait_recv()


def kernel(
    tokens_ref, gain_ref, wq_ref, wk_ref, wv_ref, wo_ref,
    mixed_ref, logs_ref,
    raw, normed, weights, w_out, queries, kv0, kv1, kv2, bias, heads, gathered,
    own_logs, partner_logs, send_sem, recv_sem, local_sem,
):
    s, x = lax.axis_index("sp"), lax.axis_index("tp")
    c, q = s % 2, s // 2
    y, z = q % 4, q // 4
    kv = (kv0, kv1, kv2)
    send = Sender(send_sem, recv_sem)

    def at(chip, core, column):
        return (chip * 2 + core, column)

    def chip_of(a, b):
        return (1 - c) * (b * 4 + a) + c * (a * 4 + b)

    a, b = (1 - c) * y + c * z, (1 - c) * z + c * y
    to_a = {d: at(chip_of((a + d + 4) % 4, b), c, x) for d in (1, -1)}
    to_b = {d: at(chip_of(a, (b + d + 4) % 4), c, x) for d in (1, -1)}
    xs = {d: (x + d + 4) % 4 for d in (1, -1, 2)}
    to_x = {d: at(q, c, xs[d]) for d in (1, -1, 2)}
    partner = at(q, 1 - c, x)
    onward, behind = at((q + 1) % 16, c, x), at((q + 15) % 16, c, x)

    def local(src, dst, slot):
        copy = pltpu.make_async_copy(src, dst, local_sem.at[slot])
        copy.start()
        return copy

    load = local(tokens_ref, raw, 0)
    mine = pl.ds(pl.multiple_of(q * 128 + c * 64, 64), 64)
    roles = (wk_ref, wv_ref, wq_ref)
    own_columns = pl.ds(pl.multiple_of(c * HEAD, HEAD), HEAD)
    other_columns = pl.ds(pl.multiple_of((1 - c) * HEAD, HEAD), HEAD)
    kept = {}
    for g in (2, 1, 0):
        for r, ref in enumerate(roles):
            kept[g, r] = local(
                ref.at[g, :, own_columns],
                weights.at[g, mine, pl.ds(r * HEAD, HEAD)],
                1 + g * 3 + r,
            )
    x_columns = {d: pl.ds(pl.multiple_of(((x + d + 4) % 4) * 256, 256), 256) for d in (0, 1, -1, 2)}
    kept_out = local(wo_ref, w_out.at[q, c, :, x_columns[0]], 10)

    barrier = pltpu.get_barrier_semaphore()
    peers = [partner, to_a[1], to_a[-1], to_b[1], to_b[-1], onward, behind]
    for d in (1, -1, 2):
        peers += [at(q, c, xs[d]), at(q, 1 - c, xs[d])]
    for peer in peers:
        pl.semaphore_signal(barrier, inc=1, device_id=peer, device_id_type=MESH)
    pl.semaphore_wait(barrier, len(peers))

    swapped = {}
    for g in (2, 1, 0):
        for r, ref in enumerate(roles):
            swapped[g, r] = send(
                ref.at[g, :, other_columns],
                weights.at[g, mine, pl.ds(r * HEAD, HEAD)],
                partner,
            )

    def slab(core, column):
        return pl.ds(pl.multiple_of(core * 128 + column * PIECE, PIECE), PIECE)

    load.wait()
    own_slab = slab(c, x)

    def norm_one(i, _):
        wide = raw[i].astype(F32)
        mean = jnp.sum(wide * wide, axis=-1, keepdims=True) * (1.0 / WIDTH)
        scaled = wide * lax.rsqrt(mean + EPSILON)
        normed[i, own_slab, :] = (scaled * gain_ref[...]).astype(BF16)
        return 0

    lax.fori_loop(0, BATCH, norm_one, 0)

    halves = (pl.ds(0, 3), pl.ds(3, 3))

    def tokens_of(half, column):
        return normed.at[halves[half], slab(c, column), :]

    ring, mirrored = {}, []
    for step in range(2):
        for side in (1, -1):
            half = step if side == 1 else 1 - step
            ref = tokens_of(half, x)
            ring[side, half] = send(ref, ref, to_x[side])
        ref = tokens_of(step, x)
        mirrored.append(send(ref, ref, partner))

    def mirror(half, column):
        ref = tokens_of(half, column)
        copy = send(ref, ref, partner)
        mirrored.append(copy)
        return copy

    def block_of(g):
        def block(ba, bb, half):
            row = chip_of(ba, bb) * 128
            if half is None:
                return weights.at[g, pl.ds(pl.multiple_of(row, 128), 128), :]
            return weights.at[g, pl.ds(pl.multiple_of(row + 64 * half, 64), 64), :]

        return block

    def out_block(ba, bb, half):
        chip = chip_of(ba, bb)
        if half is None:
            return w_out.at[chip, c, :, x_columns[0]]
        return w_out.at[chip, c, pl.ds(32 * half, 32), x_columns[0]]

    plane = [PlaneGather(send, block_of(g), a, b, to_a, to_b) for g in range(3)]
    plane_out = PlaneGather(send, out_block, a, b, to_a, to_b)

    def begin(g):
        for r in range(3):
            kept[g, r].wait()
            swapped[g, r].wait_recv()
        plane[g].begin()

    def project(g, deltas):
        def one(i, _):
            core = i % 2
            column = (x + deltas[0] + i // 2 + 4) % 4
            rows = normed[:, slab(core, column), :].reshape(BATCH * PIECE, WIDTH)
            product = jnp.dot(rows, weights[g], preferred_element_type=F32).astype(BF16)
            product = product.reshape(BATCH, PIECE, 3 * HEAD)
            start = core * 128 + column * PIECE
            kv[g][:, pl.ds(pl.multiple_of(HALO[g] + start, PIECE), PIECE), :] = product[:, :, : 2 * HEAD]
            queries[g, :, pl.ds(pl.multiple_of(start, PIECE), PIECE), :] = product[:, :, 2 * HEAD :]
            return 0

        lax.fori_loop(0, 2 * len(deltas), one, 0)

    wide_sent = {}

    def send_wide(d):
        column = (x + d + 4) % 4
        for core in (1, 0):
            start = core * 128 + column * PIECE
            wide_sent[core, d] = send(
                kv2.at[:, pl.ds(pl.multiple_of(384 + start, PIECE), PIECE), :],
                kv2.at[:, pl.ds(pl.multiple_of(128 + start, PIECE), PIECE), :],
                onward,
            )

    def forward_wide(d):
        column = (x + d + 4) % 4
        wide_sent[1, d].wait_recv()
        return send(
            kv2.at[:, pl.ds(pl.multiple_of(256 + column * PIECE, PIECE), PIECE), :],
            kv2.at[:, pl.ds(pl.multiple_of(column * PIECE, PIECE), PIECE), :],
            onward,
        )

    begin(2)
    plane[2].first()
    begin(1)
    plane[2].second()
    plane[2].third()
    plane[1].first()

    own_logs[...] = jnp.zeros_like(own_logs)

    for half in range(2):
        row = 0
        for g in (2, 1, 0):
            key = lax.broadcasted_iota(jnp.int32, (SPAN[g], 128), 0)
            lane = lax.broadcasted_iota(jnp.int32, (SPAN[g], 128), 1)
            lag = lane - key + HALO[g]
            position = key + (half * 128 - HALO[g]) + q * ROWS
            seen = (lag >= 0) & (lag <= STEPS * DILATION[g]) & (position >= 0)
            if DILATION[g] > 1:
                seen = seen & ((lag & (DILATION[g] - 1)) == 0)
            bias[half, row : row + SPAN[g], :] = jnp.where(seen, F32(0), F32(-1e30))
            row += SPAN[g]

    ring[1, 0].wait_recv()
    far = {1: send(tokens_of(0, xs[-1]), tokens_of(0, xs[-1]), to_x[1])}
    mirror(0, xs[-1])
    ring[-1, 1].wait_recv()
    far[-1] = send(tokens_of(1, xs[1]), tokens_of(1, xs[1]), to_x[-1])
    mirror(1, xs[1])
    plane[2].finish()
    begin(0)
    for copy in mirrored[:2]:
        copy.wait_recv()
    project(2, (0,))
    send_wide(0)
    plane[1].second()
    plane[1].third()
    plane[0].first()
    kept_out.wait()
    plane_out.begin()
    ring[1, 1].wait_recv()
    mirror(1, xs[-1])
    ring[-1, 0].wait_recv()
    mirror(0, xs[1])
    plane[1].finish()
    for copy in mirrored[2:6]:
        copy.wait_recv()
    project(2, (1,))
    send_wide(1)
    project(2, (-1,))
    send_wide(-1)
    plane[0].second()
    project(1, (-1, 0, 1))
    plane[0].third()
    plane_out.first()
    plane_out.second()
    plane_out.third()
    far[1].wait_recv()
    mirror(0, xs[2])
    far[-1].wait_recv()
    mirror(1, xs[2])
    for copy in mirrored[6:]:
        copy.wait_recv()
    project(2, (2,))
    send_wide(2)
    project(1, (2,))
    middle = send(kv1.at[:, pl.ds(ROWS, 96), :], kv1.at[:, pl.ds(0, 96), :], onward)
    plane_out.finish()
    out_halves = (pl.ds(0, 8), pl.ds(8, 8))

    def out_of(half, d):
        return w_out.at[out_halves[half], c, :, x_columns[d]]

    out_ring = {}
    for step in range(2):
        for side in (1, -1):
            half = step if side == 1 else 1 - step
            out_ring[side, half] = send(out_of(half, 0), out_of(half, 0), to_x[side])
    out_mirror = []

    def mirror_out(d):
        ref = w_out.at[:, c, :, x_columns[d]]
        out_mirror.append(send(ref, ref, partner))

    mirror_out(0)
    plane[0].finish()
    project(0, (-1, 0, 1, 2))
    near = send(kv0.at[:, pl.ds(ROWS, 32), :], kv0.at[:, pl.ds(0, 32), :], onward)
    late = [forward_wide(d) for d in (0, 1, -1, 2)]
    out_far = {}
    for side, half in ((1, 0), (-1, 1)):
        out_ring[side, half].wait_recv()
        out_far[side] = send(out_of(half, -side), out_of(half, -side), to_x[side])
    for side, half in ((1, 1), (-1, 0)):
        out_ring[side, half].wait_recv()
        mirror_out(-side)
    for d in (0, 1, -1, 2):
        wide_sent[0, d].wait_recv()
    middle.wait_recv()
    near.wait_recv()
    for copy in late:
        copy.wait_recv()

    scale = 1.0 / math.sqrt(HEAD)
    column_of_mine = pl.ds(pl.multiple_of((2 * x + c) * HEAD, HEAD), HEAD)
    for half in range(2):

        def attend(i, _):
            parts, row = [], 0
            for g in (2, 1, 0):
                keys = kv[g][i, pl.ds(half * 128, SPAN[g]), pl.ds(0, HEAD)]
                query = queries[g, i, pl.ds(half * 128, 128), :]
                score = lax.dot_general(keys, query, NT, preferred_element_type=F32)
                parts.append(score * scale + bias[half, row : row + SPAN[g], :])
                row += SPAN[g]
            peak = functools.reduce(jnp.maximum, [jnp.max(p, axis=0, keepdims=True) for p in parts])
            total = jnp.zeros((1, 128), F32)
            mixture = jnp.zeros((HEAD, 128), F32)
            for g, part in zip((2, 1, 0), parts):
                lifted = jnp.exp(part - peak)
                total = total + jnp.sum(lifted, axis=0, keepdims=True)
                values = kv[g][i, pl.ds(half * 128, SPAN[g]), pl.ds(HEAD, HEAD)]
                mixture = mixture + lax.dot_general(
                    values, lifted.astype(BF16), TN, preferred_element_type=F32
                )
            own_logs[half, pl.ds(i, 1), :] = peak + jnp.log(total)
            heads[i, pl.ds(half * 128, 128), :] = (mixture / total).T.astype(BF16)
            return 0

        lax.fori_loop(0, BATCH, attend, 0)
        if half == 1:
            logs_copy = send(own_logs.at[1 - c], partner_logs, partner)
            copies = []
            for d in (2, 1, -1):
                for core in (c, 1 - c):
                    copies.append(
                        send(
                            heads.at[:, slab(core, xs[d]), :],
                            gathered.at[:, :, column_of_mine],
                            at(q, core, xs[d]),
                        )
                    )
            copies.append(
                send(heads.at[:, slab(1 - c, x), :], gathered.at[:, :, column_of_mine], partner)
            )
            stay = local(heads.at[:, slab(c, x), :], gathered.at[:, :, column_of_mine], 11)
    for side in (1, -1):
        out_far[side].wait_recv()
    mirror_out(2)
    logs_copy.wait_recv()
    mine_logs, their_logs = own_logs[c], partner_logs[...]
    first = jnp.where(c == 0, mine_logs, their_logs)
    second = jnp.where(c == 0, their_logs, mine_logs)
    logs_ref[:, 0, :] = first[:BATCH]
    logs_ref[:, 1, :] = second[:BATCH]
    for copy in copies:
        copy.wait_recv()
    stay.wait()
    for copy in out_mirror:
        copy.wait_recv()

    combined = gathered[...].reshape(BATCH * PIECE, 8 * HEAD)

    def out_tile(i, _):
        tile = w_out[pl.ds(i * 4, 4)].reshape(512, 8 * HEAD)
        product = lax.dot_general(combined, tile, NT, preferred_element_type=F32)
        columns = pl.ds(pl.multiple_of(i * 512, 512), 512)
        mixed_ref[:, :, columns] = product.astype(BF16).reshape(BATCH, PIECE, 512)
        return 0

    lax.fori_loop(0, 4, out_tile, 0)
    for copy in send.started:
        copy.wait_send()


def layer(tokens, norm_gain, w_query, w_key, w_value, w_out):
    any_space = pl.BlockSpec(memory_space=pl.ANY)
    vmem = pl.BlockSpec(memory_space=pltpu.VMEM)
    mixed, logs = pl.pallas_call(
        kernel,
        out_shape=(
            jax.ShapeDtypeStruct((BATCH, PIECE, WIDTH), BF16),
            jax.ShapeDtypeStruct((BATCH, 2, 128), F32),
        ),
        in_specs=[any_space, vmem, any_space, any_space, any_space, any_space],
        out_specs=(vmem, vmem),
        scratch_shapes=[
            pltpu.VMEM((BATCH, PIECE, WIDTH), BF16),
            pltpu.VMEM((BATCH, ROWS, WIDTH), BF16),
            pltpu.VMEM((3, WIDTH, 3 * HEAD), BF16),
            pltpu.VMEM((16, 2, 64, 8 * HEAD), BF16),
            pltpu.VMEM((3, BATCH, ROWS, HEAD), BF16),
            pltpu.VMEM((BATCH, HALO[0] + ROWS, 2 * HEAD), BF16),
            pltpu.VMEM((BATCH, HALO[1] + ROWS, 2 * HEAD), BF16),
            pltpu.VMEM((BATCH, HALO[2] + ROWS, 2 * HEAD), BF16),
            pltpu.VMEM((2, sum(SPAN), 128), F32),
            pltpu.VMEM((BATCH, ROWS, HEAD), BF16),
            pltpu.VMEM((BATCH, PIECE, 8 * HEAD), BF16),
            pltpu.VMEM((2, 8, 128), F32),
            pltpu.VMEM((8, 128), F32),
            pltpu.SemaphoreType.DMA((COPIES,)),
            pltpu.SemaphoreType.DMA((COPIES,)),
            pltpu.SemaphoreType.DMA((12,)),
        ],
        compiler_params=pltpu.CompilerParams(
            collective_id=0, has_side_effects=True, vmem_limit_bytes=56 * 1024 * 1024
        ),
    )(
        jnp.transpose(tokens, (1, 0, 2)),
        norm_gain.reshape(1, WIDTH),
        w_query,
        w_key,
        w_value,
        jnp.transpose(w_out),
    )
    return jnp.transpose(mixed, (1, 0, 2)), jnp.transpose(logs, (2, 0, 1))


def solution(mesh):
    in_specs = (
        P(("sp", "tp"), None, None),
        P(),
        P(None, "sp", "tp"),
        P(None, "sp", "tp"),
        P(None, "sp", "tp"),
        P("tp", "sp"),
    )
    out_specs = (P(("sp", "tp"), None, None), P("sp", None, "tp"))
    return jax.shard_map(layer, mesh=mesh, in_specs=in_specs, out_specs=out_specs, check_vma=False)
```

time: 262 us -> 109 us (0.42)
  the two profiles are of different devices: /device:TPU:0 before, /device:TPU:41 now
where the time goes in v1:
time: 109 us
  Pallas kernels  106 us (97%)
  local copies, waits for them, and re-layouts  2.69 us (2%)
    pallas_call x1, Pallas kernels, layer(): pl.pallas_call(kernel, out_shape=(jax.ShapeDtypeStruct((BATCH, PIECE, WID...  106 us
    unnamed x4, local copies, waits for them, and re-layouts  2.69 us

profile of v1, /device:TPU:41, one launch (start us, length us, event | category | flops | bytes accessed | tf_op | source)
XLA Modules:
  0.0 109.3 jit_solution(4208267225903890600)
XLA Ops:
  0.6 105.9 %shard_map.77 = (bf16[6,32,2048]{2,1,0:T(8,128)(2,1)}, f32[6,2,128]{2,1,0:T(2,128)}) custom-call(bf16[6,32,2048]{2,1,0:T(8,128)(2,1)} %bitcast.5, f32[1,2048]{1,0:T(1,128)} %bitcast.8, bf16[3,64,256]{2,1,0:T(8,128)(2,1)} %wq_ref.1, bf16[3,64,256]{2,1,0:T(8,128)(2,1)} %wk_ref.1, bf16[3,64,256]{2,1,0:T(8,128)(2,1)} %wv_ref.1, bf16[64,256]{1,0:T(8,128)(2,1)} %bitcast.7), custom_call_target="tpu_custom_call" | custom-call | tf_op jit(solution)/shard_map/pallas_call | solution.py:426
  106.6 0.0 copy-start
  106.6 2.1 %copy.10 = bf16[32,6,2048]{2,0,1:T(8,128)(2,1)} copy(bf16[32,6,2048]{2,0,1:T(8,128)(2,1)} %bitcast.6) | data formatting | bytes 1572864
  108.7 0.0 copy-done
  108.7 0.6 copy.11
Async XLA Ops:
  106.6 2.1 %copy-start = (f32[6,2,128]{2,1,0:T(2,128)S(1)}, f32[6,2,128]{2,1,0:T(2,128)}, u32[]{:S(2)}) copy-start(f32[6,2,128]{2,1,0:T(2,128)} %get-tuple-element.5) | copy-start | bytes 18436

commit v2 on v1

v2 whole, which is shorter than its diff:
```python
import functools
import math

import jax
import jax.numpy as jnp
from jax import lax
from jax.experimental import pallas as pl
from jax.experimental.pallas import tpu as pltpu
from jax.sharding import PartitionSpec as P

MESH = pl.DeviceIdType.MESH
BATCH = 6
WIDTH = 2048
HEAD = 128
STEPS = 24
EPSILON = 1e-06
ROWS = 256
PIECE = 32
HALO = (32, 96, 384)
SPAN = (160, 224, 512)
DILATION = (1, 4, 16)
COPIES = 200
EXCHANGE = 192
F32 = jnp.float32
BF16 = jnp.bfloat16
DELTAS = (0, 1, -1, 2)
LOPSIDED = ('kv0', 'q')
NT = (((1,), (1,)), ((), ()))
TN = (((0,), (0,)), ((), ()))


class Steps:
    pass


class Sender:
    def __init__(self, send_sem, recv_sem):
        self.send_sem, self.recv_sem, self.started = send_sem, recv_sem, []

    def __call__(self, src, dst, device):
        slot = len(self.started)
        copy = pltpu.make_async_remote_copy(
            src_ref=src,
            dst_ref=dst,
            send_sem=self.send_sem.at[slot],
            recv_sem=self.recv_sem.at[slot],
            device_id=device,
            device_id_type=MESH,
        )
        copy.start()
        self.started.append(copy)
        return copy


def plane_tasks(k, lopsided):
    if not lopsided:
        tasks = [
            ("begin", (), [("A+", 0, 0, None, "A+"), ("A-", 0, 0, None, "A-"), ("B+0", 0, 0, None, "B+"), ("B-0", 0, 0, None, "B-")]),
            ("up", ("A+",), [("A++", -1, 0, 0, "A+"), ("B+-1", -1, 0, None, "B+"), ("B--1", -1, 0, None, "B-")]),
            ("down", ("A-",), [("A--", 1, 0, 1, "A-"), ("B+1", 1, 0, None, "B+"), ("B-1", 1, 0, None, "B-")]),
            ("far", ("A++", "A--"), [("B+2", 2, 0, None, "B+"), ("B-2", 2, 0, None, "B-")]),
            ("up0", ("B+0",), [("C0", 0, -1, None, "B+")]),
            ("up3", ("B+-1",), [("C-1", -1, -1, None, "B+")]),
            ("down1", ("B-1",), [("C1", 1, 1, None, "B-")]),
            ("down2", ("B-2",), [("C2", 2, 1, None, "B-")]),
            ("finish", ("B-0", "B--1", "B+1", "B+2", "C0", "C-1", "C1", "C2"), []),
        ]
    else:
        def spread(d):
            return [(f"B-{d}", d, 0, None, "B-"), (f"B+{d}", d, 0, 0, "B+")]

        tasks = [
            ("begin", (), [("A-", 0, 0, None, "A-"), ("A+", 0, 0, 0, "A+"), *spread(0)]),
            ("one", ("A-",), [("A--", 1, 0, None, "A-"), *spread(1)]),
            ("two", ("A--",), [("A---", 2, 0, 1, "A-"), *spread(2)]),
            ("back", ("A+", "A---"), spread(-1)),
        ]
        for d in DELTAS:
            tasks.append((f"next{d % 4}", (f"B-{d}",), [(f"C{d}", d, 1, None, "B-")]))
            tasks.append((f"last{d % 4}", (f"C{d}",), [(f"D{d}", d, 2, 1, "B-")]))
        tasks.append(("finish", tuple(f"{w}{d}" for d in DELTAS for w in ("B+", "D")), []))
    return [
        (f"{k}.{n}", tuple(f"{k}.{w}" for w in needs), [(f"{k}.{key}", *rest) for key, *rest in starts])
        for n, needs, starts in tasks
    ]


def kernel(
    tokens_ref, gain_ref, wq_ref, wk_ref, wv_ref, wo_ref,
    mixed_ref, logs_ref,
    raw, normed, w_kv, w_q, w_out, queries, kv0, kv1, kv2, bias, heads, gathered,
    own_logs, partner_logs, send_sem, recv_sem, local_sem,
):
    s, x = lax.axis_index("sp"), lax.axis_index("tp")
    c, q = s % 2, s // 2
    y, z = q % 4, q // 4
    kv = (kv0, kv1, kv2)
    send = Sender(send_sem, recv_sem)
    tok, out, wide = Steps(), Steps(), Steps()
    kv2_part, kv1_part, kv0_part, q_part, wo_part = (Steps() for _ in range(5))
    parts = {"kv2": kv2_part, "kv1": kv1_part, "kv0": kv0_part, "q": q_part, "wo": wo_part}

    def at(chip, core, column):
        return (chip * 2 + core, column)

    def chip_of(a, b):
        return (1 - c) * (b * 4 + a) + c * (a * 4 + b)

    a, b = (1 - c) * y + c * z, (1 - c) * z + c * y
    xs = {d: (x + d + 4) % 4 for d in (0, 1, -1, 2)}
    partner = at(q, 1 - c, x)
    onward, behind = at((q + 1) % 16, c, x), at((q + 15) % 16, c, x)
    ways = {
        "A+": at(chip_of((a + 1) % 4, b), c, x),
        "A-": at(chip_of((a + 3) % 4, b), c, x),
        "B+": at(chip_of(a, (b + 1) % 4), c, x),
        "B-": at(chip_of(a, (b + 3) % 4), c, x),
        "x+": at(q, c, xs[1]),
        "x-": at(q, c, xs[-1]),
        "p": partner,
        "h": onward,
    }

    sent, seen = {}, set()

    def start(key, src, dst, way):
        sent[key] = send(src, dst, ways[way])

    def arrived(*keys):
        for key in keys:
            if key not in seen:
                seen.add(key)
                sent[key].wait_recv()

    def local(src, dst, slot):
        copy = pltpu.make_async_copy(src, dst, local_sem.at[slot])
        copy.start()
        return copy

    load = local(tokens_ref, raw, 0)
    mine = pl.ds(pl.multiple_of(q * 128 + c * 64, 64), 64)
    own_columns = pl.ds(pl.multiple_of(c * HEAD, HEAD), HEAD)
    other_columns = pl.ds(pl.multiple_of((1 - c) * HEAD, HEAD), HEAD)
    swaps = []
    for g in (2, 1, 0):
        for r, ref in enumerate((wk_ref, wv_ref)):
            swaps.append((f"kv{g}", ref.at[g], w_kv.at[g, mine, pl.ds(r * HEAD, HEAD)]))
    for g in range(3):
        swaps.append(("q", wq_ref.at[g], w_q.at[mine, pl.ds(g * HEAD, HEAD)]))
    kept = {}
    for i, (k, src, dst) in enumerate(swaps):
        kept.setdefault(k, []).append(local(src.at[:, own_columns], dst, 1 + i))
    x_columns = {d: pl.ds(pl.multiple_of(xs[d] * 256, 256), 256) for d in DELTAS}
    kept["wo"] = [local(wo_ref, w_out.at[q, c, :, x_columns[0]], 10)]

    barrier = pltpu.get_barrier_semaphore()
    peers = [partner, onward, behind] + [ways[w] for w in ("A+", "A-", "B+", "B-")]
    for d in (1, -1, 2):
        peers += [at(q, c, xs[d]), at(q, 1 - c, xs[d])]
    for peer in peers:
        pl.semaphore_signal(barrier, inc=1, device_id=peer, device_id_type=MESH)
    pl.semaphore_wait(barrier, len(peers))

    swapped = {"wo": []}
    for i, (k, src, dst) in enumerate(swaps):
        start(f"swap{i}", src.at[:, other_columns], dst, "p")
        swapped.setdefault(k, []).append(f"swap{i}")

    def slab(core, column):
        return pl.ds(pl.multiple_of(core * 128 + column * PIECE, PIECE), PIECE)

    halves = (pl.ds(0, 3), pl.ds(3, 3))

    def pass_on(key, half, d, way):
        ref = normed.at[halves[half], slab(c, xs[d]), :]
        start(key, ref, ref, way)

    def norm():
        load.wait()
        own_slab = slab(c, x)

        def one(i, _):
            wide = raw[i].astype(F32)
            mean = jnp.sum(wide * wide, axis=-1, keepdims=True) * (1.0 / WIDTH)
            scaled = wide * lax.rsqrt(mean + EPSILON)
            normed[i, own_slab, :] = (scaled * gain_ref[...]).astype(BF16)
            return 0

        lax.fori_loop(0, BATCH, one, 0)
        for half in range(2):
            pass_on(f"x+{half}", half, 0, "x+")
            pass_on(f"x-{1 - half}", 1 - half, 0, "x-")
            pass_on(f"p{half}", half, 0, "p")

    def token_step(needs, starts):
        def run():
            arrived(needs)
            for args in starts:
                pass_on(*args)

        return run

    tok.begin = norm
    tok.a = token_step("x+0", [("x++", 0, -1, "x+"), ("m-1.0", 0, -1, "p")])
    tok.b = token_step("x-1", [("x--", 1, 1, "x-"), ("m1.1", 1, 1, "p")])
    tok.c = token_step("x+1", [("m-1.1", 1, -1, "p")])
    tok.d = token_step("x-0", [("m1.0", 0, 1, "p")])
    tok.e = token_step("x++", [("m2.0", 0, 2, "p")])
    tok.f = token_step("x--", [("m2.1", 1, 2, "p")])
    token_needs = {0: ("p0", "p1")}
    token_needs[-1] = ("x+0", "x+1", "m-1.0", "m-1.1")
    token_needs[1] = ("x-0", "x-1", "m1.0", "m1.1")
    token_needs[2] = ("x++", "x--", "m2.0", "m2.1")

    def block(k, da, db, half):
        chip = chip_of((a + da + 4) % 4, (b + db + 4) % 4)
        if k == "wo":
            rows = pl.ds(0, 64) if half is None else pl.ds(32 * half, 32)
            return w_out.at[chip, c, rows, x_columns[0]]
        if half is None:
            rows = pl.ds(pl.multiple_of(chip * 128, 128), 128)
        else:
            rows = pl.ds(pl.multiple_of(chip * 128 + 64 * half, 64), 64)
        return w_q.at[rows, :] if k == "q" else w_kv.at[int(k[2]), rows, :]

    def plane_step(k, name, needs, starts):
        def run():
            if name.endswith("begin"):
                for copy in kept[k]:
                    copy.wait()
                arrived(*swapped[k])
            arrived(*needs)
            for key, da, db, half, way in starts:
                ref = block(k, da, db, half)
                start(key, ref, ref, way)

        return run

    for k in ("kv2", "kv1", "kv0", "q", "wo"):
        for name, needs, starts in plane_tasks(k, k in LOPSIDED):
            setattr(parts[k], name.split(".")[1], plane_step(k, name, needs, starts))

    out_halves = (pl.ds(0, 8), pl.ds(8, 8), pl.ds(0, 16))

    def pass_out(key, half, d, way):
        ref = w_out.at[out_halves[half], c, :, x_columns[d]]
        start(key, ref, ref, way)

    def out_step(needs, starts):
        def run():
            arrived(*needs)
            for args in starts:
                pass_out(*args)

        return run

    out.begin = out_step((), [
        ("o+0", 0, 0, "x+"), ("o-1", 1, 0, "x-"), ("o+1", 1, 0, "x+"), ("o-0", 0, 0, "x-"), ("n0", 2, 0, "p")
    ])
    out.a = out_step(("o+0",), [("o++", 0, -1, "x+")])
    out.b = out_step(("o-1",), [("o--", 1, 1, "x-")])
    out.c = out_step(("o+0", "o+1"), [("n-1", 2, -1, "p")])
    out.d = out_step(("o-0", "o-1"), [("n1", 2, 1, "p")])
    out.e = out_step(("o++", "o--"), [("n2", 2, 2, "p")])

    def rows_of(i, d):
        return normed[:, slab(i, xs[d]), :].reshape(BATCH * PIECE, WIDTH)

    def project_kv(g, d):
        def one(i, _):
            product = jnp.dot(rows_of(i, d), w_kv[g], preferred_element_type=F32).astype(BF16)
            first = pl.multiple_of(HALO[g] + i * 128 + xs[d] * PIECE, PIECE)
            kv[g][:, pl.ds(first, PIECE), :] = product.reshape(BATCH, PIECE, 2 * HEAD)
            return 0

        def run():
            arrived(*token_needs[d])
            lax.fori_loop(0, 2, one, 0)
            if g == 2:
                for core in (1, 0):
                    first = core * 128 + xs[d] * PIECE
                    start(
                        f"w{core}.{d}",
                        kv2.at[:, pl.ds(pl.multiple_of(384 + first, PIECE), PIECE), :],
                        kv2.at[:, pl.ds(pl.multiple_of(128 + first, PIECE), PIECE), :],
                        "h",
                    )

        return run

    def project_q(d):
        def one(i, _):
            product = jnp.dot(rows_of(i, d), w_q[...], preferred_element_type=F32).astype(BF16)
            for g in range(3):
                part = product[:, g * HEAD : (g + 1) * HEAD].reshape(BATCH, PIECE, HEAD)
                queries[g, :, slab(i, xs[d]), :] = part
            return 0

        def run():
            arrived(*token_needs[d])
            lax.fori_loop(0, 2, one, 0)

        return run

    def forward_wide(d):
        def run():
            arrived(f"w1.{d}")
            start(
                f"f.{d}",
                kv2.at[:, pl.ds(pl.multiple_of(256 + xs[d] * PIECE, PIECE), PIECE), :],
                kv2.at[:, slab(0, xs[d]), :],
                "h",
            )

        return run

    for d in DELTAS:
        for g in range(3):
            setattr(parts[f"kv{g}"], f"project{d % 4}", project_kv(g, d))
        setattr(q_part, f"project{d % 4}", project_q(d))
        setattr(wide, f"onward{d % 4}", forward_wide(d))
    kv1_part.halo = lambda: start("mid", kv1.at[:, pl.ds(ROWS, 96), :], kv1.at[:, pl.ds(0, 96), :], "h")
    kv0_part.halo = lambda: start("near", kv0.at[:, pl.ds(ROWS, 32), :], kv0.at[:, pl.ds(0, 32), :], "h")

    def make_masks():
        own_logs[...] = jnp.zeros_like(own_logs)
        for half in range(2):
            row = 0
            for g in (2, 1, 0):
                key = lax.broadcasted_iota(jnp.int32, (SPAN[g], 128), 0)
                lane = lax.broadcasted_iota(jnp.int32, (SPAN[g], 128), 1)
                lag = lane - key + HALO[g]
                position = key + (half * 128 - HALO[g]) + q * ROWS
                met = (lag >= 0) & (lag <= STEPS * DILATION[g]) & (position >= 0)
                if DILATION[g] > 1:
                    met = met & ((lag & (DILATION[g] - 1)) == 0)
                bias[half, row : row + SPAN[g], :] = jnp.where(met, F32(0), F32(-1e30))
                row += SPAN[g]

    scale = 1.0 / math.sqrt(HEAD)
    column_of_mine = pl.ds(pl.multiple_of((2 * x + c) * HEAD, HEAD), HEAD)

    def attend(half):
        def one(i, _):
            parts, row = [], 0
            for g in (2, 1, 0):
                keys = kv[g][i, pl.ds(half * 128, SPAN[g]), pl.ds(0, HEAD)]
                query = queries[g, i, pl.ds(half * 128, 128), :]
                score = lax.dot_general(keys, query, NT, preferred_element_type=F32)
                parts.append(score * scale + bias[half, row : row + SPAN[g], :])
                row += SPAN[g]
            peak = functools.reduce(jnp.maximum, [jnp.max(p, axis=0, keepdims=True) for p in parts])
            total = jnp.zeros((1, 128), F32)
            mixture = jnp.zeros((HEAD, 128), F32)
            for g, part in zip((2, 1, 0), parts):
                lifted = jnp.exp(part - peak)
                total = total + jnp.sum(lifted, axis=0, keepdims=True)
                values = kv[g][i, pl.ds(half * 128, SPAN[g]), pl.ds(HEAD, HEAD)]
                mixture = mixture + lax.dot_general(
                    values, lifted.astype(BF16), TN, preferred_element_type=F32
                )
            own_logs[half, pl.ds(i, 1), :] = peak + jnp.log(total)
            heads[i, pl.ds(half * 128, 128), :] = (mixture / total).T.astype(BF16)
            return 0

        lax.fori_loop(0, BATCH, one, 0, unroll=2)

    exchanged = []

    def exchange(half):
        for i, d in enumerate((2, 1, -1)):
            copy = pltpu.make_async_remote_copy(
                src_ref=heads.at[:, slab(half, xs[d]), :],
                dst_ref=gathered.at[:, :, column_of_mine],
                send_sem=send_sem.at[EXCHANGE + 2 * i + half],
                recv_sem=recv_sem.at[EXCHANGE + 2 * i + c],
                device_id=at(q, half, xs[d]),
                device_id_type=MESH,
            )
            copy.start()
            exchanged.append(copy)

    make_masks()
    order = (
        tok.begin, kv2_part.begin, kv1_part.begin, kv2_part.up, kv2_part.down, kv2_part.up0,
        kv1_part.up, kv1_part.down, kv1_part.up0, kv2_part.far, kv2_part.up3, kv2_part.down1,
        kv1_part.far, kv0_part.begin, wo_part.begin, kv1_part.up3, kv1_part.down1, kv2_part.down2,
        tok.a, tok.b, kv0_part.one, wo_part.up, wo_part.down, kv1_part.down2,
        kv0_part.next0, wo_part.up0, q_part.begin, kv0_part.two, wo_part.far, kv2_part.finish,
        wo_part.up3, kv2_part.project0, kv0_part.next1, wo_part.down1, q_part.one, tok.c,
        tok.d, kv0_part.back, kv1_part.finish, kv1_part.project0, kv0_part.last0, kv2_part.project3,
        wide.onward0, q_part.next0, kv2_part.project1, q_part.two, kv0_part.next2, kv1_part.project1,
        wo_part.down2, kv1_part.project3, kv0_part.last1, q_part.next1, q_part.back, kv0_part.next3,
        wide.onward3, tok.e, tok.f, q_part.last0, q_part.next2, kv0_part.last2,
        wo_part.finish, out.begin, kv2_part.project2, kv1_part.project2, kv1_part.halo, q_part.last1,
        q_part.next3, kv0_part.last3, wide.onward1, q_part.last2, q_part.last3, kv0_part.finish,
        kv0_part.project0, out.a, out.b, kv0_part.project1, kv0_part.project3, q_part.finish,
        kv0_part.project2, kv0_part.halo, wide.onward2, q_part.project0, q_part.project1, q_part.project3,
        out.c, out.d, q_part.project2, out.e,
    )
    for step in order:
        step()

    arrived(*(f"w{core}.{d}" for core in (1, 0) for d in DELTAS), "mid", "near")
    attend(1)
    exchange(1)
    arrived(*(f"f.{d}" for d in DELTAS))
    attend(0)
    exchange(0)
    start("logs", own_logs.at[1 - c], partner_logs, "p")
    start("heads", heads.at[:, slab(1 - c, x), :], gathered.at[:, :, column_of_mine], "p")
    stay = local(heads.at[:, slab(c, x), :], gathered.at[:, :, column_of_mine], 11)
    arrived("n0", "n1", "n-1", "n2", "logs")
    mine_logs, their_logs = own_logs[c], partner_logs[...]
    logs_ref[:, 0, :] = jnp.where(c == 0, mine_logs, their_logs)[:BATCH]
    logs_ref[:, 1, :] = jnp.where(c == 0, their_logs, mine_logs)[:BATCH]
    stay.wait()
    arrived("heads")
    for slot in range(6):
        pltpu.make_async_remote_copy(
            src_ref=heads.at[:, pl.ds(0, PIECE), :],
            dst_ref=gathered.at[:, :, column_of_mine],
            send_sem=send_sem.at[EXCHANGE + slot],
            recv_sem=recv_sem.at[EXCHANGE + slot],
            device_id=partner,
            device_id_type=MESH,
        ).wait_recv()

    combined = gathered[...].reshape(BATCH * PIECE, 8 * HEAD)

    def out_tile(i, _):
        tile = w_out[pl.ds(i * 4, 4)].reshape(512, 8 * HEAD)
        product = lax.dot_general(combined, tile, NT, preferred_element_type=F32)
        columns = pl.ds(pl.multiple_of(i * 512, 512), 512)
        mixed_ref[:, :, columns] = product.astype(BF16).reshape(BATCH, PIECE, 512)
        return 0

    lax.fori_loop(0, 4, out_tile, 0)
    for copy in send.started + exchanged:
        copy.wait_send()


def layer(tokens, norm_gain, w_query, w_key, w_value, w_out):
    any_space = pl.BlockSpec(memory_space=pl.ANY)
    vmem = pl.BlockSpec(memory_space=pltpu.VMEM)
    mixed, logs = pl.pallas_call(
        kernel,
        out_shape=(
            jax.ShapeDtypeStruct((BATCH, PIECE, WIDTH), BF16),
            jax.ShapeDtypeStruct((BATCH, 2, 128), F32),
        ),
        in_specs=[any_space, vmem, any_space, any_space, any_space, any_space],
        out_specs=(vmem, vmem),
        scratch_shapes=[
            pltpu.VMEM((BATCH, PIECE, WIDTH), BF16),
            pltpu.VMEM((BATCH, ROWS, WIDTH), BF16),
            pltpu.VMEM((3, WIDTH, 2 * HEAD), BF16),
            pltpu.VMEM((WIDTH, 3 * HEAD), BF16),
            pltpu.VMEM((16, 2, 64, 8 * HEAD), BF16),
            pltpu.VMEM((3, BATCH, ROWS, HEAD), BF16),
            pltpu.VMEM((BATCH, HALO[0] + ROWS, 2 * HEAD), BF16),
            pltpu.VMEM((BATCH, HALO[1] + ROWS, 2 * HEAD), BF16),
            pltpu.VMEM((BATCH, HALO[2] + ROWS, 2 * HEAD), BF16),
            pltpu.VMEM((2, sum(SPAN), 128), F32),
            pltpu.VMEM((BATCH, ROWS, HEAD), BF16),
            pltpu.VMEM((BATCH, PIECE, 8 * HEAD), BF16),
            pltpu.VMEM((2, 8, 128), F32),
            pltpu.VMEM((8, 128), F32),
            pltpu.SemaphoreType.DMA((COPIES,)),
            pltpu.SemaphoreType.DMA((COPIES,)),
            pltpu.SemaphoreType.DMA((12,)),
        ],
        compiler_params=pltpu.CompilerParams(
            collective_id=0, has_side_effects=True, vmem_limit_bytes=56 * 1024 * 1024
        ),
    )(
        jnp.transpose(tokens, (1, 0, 2)),
        norm_gain.reshape(1, WIDTH),
        w_query,
        w_key,
        w_value,
        jnp.transpose(w_out),
    )
    return jnp.transpose(mixed, (1, 0, 2)), jnp.transpose(logs, (2, 0, 1))


def solution(mesh):
    in_specs = (
        P(("sp", "tp"), None, None),
        P(),
        P(None, "sp", "tp"),
        P(None, "sp", "tp"),
        P(None, "sp", "tp"),
        P("tp", "sp"),
    )
    out_specs = (P(("sp", "tp"), None, None), P("sp", None, "tp"))
    return jax.shard_map(layer, mesh=mesh, in_specs=in_specs, out_specs=out_specs, check_vma=False)
```

time: 109 us -> 91.1 us (0.84)
  the two profiles are of different devices: /device:TPU:41 before, /device:TPU:0 now
where the time goes in v2:
time: 91.1 us; the launch traced here: 90.9 us
  Pallas kernels  87.6 us (96%)
  local copies, waits for them, and re-layouts  2.69 us (3%)
    pallas_call x1, Pallas kernels, layer(): pl.pallas_call(kernel, out_shape=(jax.ShapeDtypeStruct((BATCH, PIECE, WID...  87.6 us
    unnamed x4, local copies, waits for them, and re-layouts  2.69 us

profile of v2, /device:TPU:0, one launch (start us, length us, event | category | flops | bytes accessed | tf_op | source)
XLA Modules:
  0.0 90.9 jit_solution(16182359559216160207)
XLA Ops:
  0.6 87.6 %shard_map.77 = (bf16[6,32,2048]{2,1,0:T(8,128)(2,1)}, f32[6,2,128]{2,1,0:T(2,128)}) custom-call(bf16[6,32,2048]{2,1,0:T(8,128)(2,1)} %bitcast.5, f32[1,2048]{1,0:T(1,128)} %bitcast.8, bf16[3,64,256]{2,1,0:T(8,128)(2,1)} %wq_ref.1, bf16[3,64,256]{2,1,0:T(8,128)(2,1)} %wk_ref.1, bf16[3,64,256]{2,1,0:T(8,128)(2,1)} %wv_ref.1, bf16[64,256]{1,0:T(8,128)(2,1)} %bitcast.7), custom_call_target="tpu_custom_call" | custom-call | tf_op jit(solution)/shard_map/pallas_call | solution.py:446
  88.2 0.0 copy-start
  88.2 2.1 %copy.10 = bf16[32,6,2048]{2,0,1:T(8,128)(2,1)} copy(bf16[32,6,2048]{2,0,1:T(8,128)(2,1)} %bitcast.6) | data formatting | bytes 1572864
  90.3 0.0 copy-done
  90.3 0.6 copy.11
Async XLA Ops:
  88.2 2.1 %copy-start = (f32[6,2,128]{2,1,0:T(2,128)S(1)}, f32[6,2,128]{2,1,0:T(2,128)}, u32[]{:S(2)}) copy-start(f32[6,2,128]{2,1,0:T(2,128)} %get-tuple-element.5) | copy-start | bytes 18436

commit v3 on v2

--- a/solution.py
+++ b/solution.py
@@ -24,7 +24,7 @@
 F32 = jnp.float32
 BF16 = jnp.bfloat16
 DELTAS = (0, 1, -1, 2)
-LOPSIDED = ('kv0', 'q')
+LEAN = {"kv2": 0, "kv1": 0, "kv0": 2, "q": 2, "wo": 2}
 NT = (((1,), (1,)), ((), ()))
 TN = (((0,), (0,)), ((), ()))
 
@@ -35,11 +35,18 @@
 
 class Sender:
     def __init__(self, send_sem, recv_sem):
-        self.send_sem, self.recv_sem, self.started = send_sem, recv_sem, []
+        self.send_sem, self.recv_sem, self.started, self.count = send_sem, recv_sem, [], 0
 
     def __call__(self, src, dst, device):
-        slot = len(self.started)
-        copy = pltpu.make_async_remote_copy(
+        copy = self.prepare(src, dst, device)
+        copy.start()
+        self.started.append(copy)
+        return copy
+
+    def prepare(self, src, dst, device):
+        slot = self.count
+        self.count += 1
+        return pltpu.make_async_remote_copy(
             src_ref=src,
             dst_ref=dst,
             send_sem=self.send_sem.at[slot],
@@ -47,13 +54,10 @@
             device_id=device,
             device_id_type=MESH,
         )
-        copy.start()
-        self.started.append(copy)
-        return copy
-
-
-def plane_tasks(k, lopsided):
-    if not lopsided:
+
+
+def plane_tasks(k, lean):
+    if lean == 0:
         tasks = [
             ("begin", (), [("A+", 0, 0, None, "A+"), ("A-", 0, 0, None, "A-"), ("B+0", 0, 0, None, "B+"), ("B-0", 0, 0, None, "B-")]),
             ("up", ("A+",), [("A++", -1, 0, 0, "A+"), ("B+-1", -1, 0, None, "B+"), ("B--1", -1, 0, None, "B-")]),
@@ -66,19 +70,24 @@
             ("finish", ("B-0", "B--1", "B+1", "B+2", "C0", "C-1", "C1", "C2"), []),
         ]
     else:
+        last = 1 if lean == 1 else None
+
         def spread(d):
-            return [(f"B-{d}", d, 0, None, "B-"), (f"B+{d}", d, 0, 0, "B+")]
-
+            up = [(f"B+{d}", d, 0, 0, "B+")] if lean == 1 else []
+            return [(f"B-{d}", d, 0, None, "B-"), *up]
+
+        first_up = [("A+", 0, 0, 0, "A+")] if lean == 1 else []
         tasks = [
-            ("begin", (), [("A-", 0, 0, None, "A-"), ("A+", 0, 0, 0, "A+"), *spread(0)]),
+            ("begin", (), [("A-", 0, 0, None, "A-"), *first_up, *spread(0)]),
             ("one", ("A-",), [("A--", 1, 0, None, "A-"), *spread(1)]),
-            ("two", ("A--",), [("A---", 2, 0, 1, "A-"), *spread(2)]),
-            ("back", ("A+", "A---"), spread(-1)),
+            ("two", ("A--",), [("A---", 2, 0, last, "A-"), *spread(2)]),
+            ("back", ("A---", "A+")[: 3 - lean], spread(-1)),
         ]
         for d in DELTAS:
             tasks.append((f"next{d % 4}", (f"B-{d}",), [(f"C{d}", d, 1, None, "B-")]))
-            tasks.append((f"last{d % 4}", (f"C{d}",), [(f"D{d}", d, 2, 1, "B-")]))
-        tasks.append(("finish", tuple(f"{w}{d}" for d in DELTAS for w in ("B+", "D")), []))
+            tasks.append((f"last{d % 4}", (f"C{d}",), [(f"D{d}", d, 2, last, "B-")]))
+        ends = ("D", "B+")[: 3 - lean]
+        tasks.append(("finish", tuple(f"{w}{d}" for d in DELTAS for w in ends), []))
     return [
         (f"{k}.{n}", tuple(f"{k}.{w}" for w in needs), [(f"{k}.{key}", *rest) for key, *rest in starts])
         for n, needs, starts in tasks
@@ -207,10 +216,13 @@
     tok.d = token_step("x-0", [("m1.0", 0, 1, "p")])
     tok.e = token_step("x++", [("m2.0", 0, 2, "p")])
     tok.f = token_step("x--", [("m2.1", 1, 2, "p")])
-    token_needs = {0: ("p0", "p1")}
-    token_needs[-1] = ("x+0", "x+1", "m-1.0", "m-1.1")
-    token_needs[1] = ("x-0", "x-1", "m1.0", "m1.1")
-    token_needs[2] = ("x++", "x--", "m2.0", "m2.1")
+
+    def token_needs(d, half):
+        if d == 0:
+            return (f"p{half}",)
+        if d == 2:
+            return (("x++", "x--")[half], f"m2.{half}")
+        return (("x-" if d == 1 else "x+") + str(half), f"m{d}.{half}")
 
     def block(k, da, db, half):
         chip = chip_of((a + da + 4) % 4, (b + db + 4) % 4)
@@ -237,7 +249,7 @@
         return run
 
     for k in ("kv2", "kv1", "kv0", "q", "wo"):
-        for name, needs, starts in plane_tasks(k, k in LOPSIDED):
+        for name, needs, starts in plane_tasks(k, LEAN[k]):
             setattr(parts[k], name.split(".")[1], plane_step(k, name, needs, starts))
 
     out_halves = (pl.ds(0, 8), pl.ds(8, 8), pl.ds(0, 16))
@@ -263,64 +275,77 @@
     out.d = out_step(("o-0", "o-1"), [("n1", 2, 1, "p")])
     out.e = out_step(("o++", "o--"), [("n2", 2, 2, "p")])
 
-    def rows_of(i, d):
-        return normed[:, slab(i, xs[d]), :].reshape(BATCH * PIECE, WIDTH)
+    def rows_of(d, part=pl.ds(0, BATCH)):
+        pieces = [normed[part, slab(core, xs[d]), :] for core in range(2)]
+        return jnp.concatenate([p.reshape(-1, WIDTH) for p in pieces], axis=0)
+
+    def need_tokens(d):
+        for half in range(2):
+            arrived(*token_needs(d, half))
+
+    def keep_kv(g, d, product, part=pl.ds(0, BATCH)):
+        product = product.astype(BF16).reshape(2, -1, PIECE, 2 * HEAD)
+        for core in range(2):
+            first = pl.multiple_of(HALO[g] + core * 128 + xs[d] * PIECE, PIECE)
+            kv[g][part, pl.ds(first, PIECE), :] = product[core]
+
+    def at_wide(half, base, core, d):
+        first = pl.multiple_of(base + core * 128 + xs[d] * PIECE, PIECE)
+        return kv2.at[halves[half], pl.ds(first, PIECE), :]
+
+    def project_wide(d, half):
+        def run():
+            arrived(*token_needs(d, half))
+            part = halves[half]
+            keep_kv(2, d, jnp.dot(rows_of(d, part), w_kv[2], preferred_element_type=F32), part)
+            for core in (1, 0):
+                start(f"w{core}{d}{half}", at_wide(half, 384, core, d), at_wide(half, 128, core, d), "h")
+
+        return run
+
+    def forward_wide(d, half):
+        def run():
+            arrived(f"w1{d}{half}")
+            start(f"f{d}{half}", at_wide(half, 256, 0, d), at_wide(half, 0, 0, d), "h")
+
+        return run
+
+    near = send.prepare(kv0.at[:, pl.ds(ROWS, 32), :], kv0.at[:, pl.ds(0, 32), :], onward)
+    middle = {}
+    for d in DELTAS:
+        to = pl.multiple_of(jnp.maximum(xs[d] - 1, 0) * PIECE, PIECE)
+        own = pl.multiple_of(96 + 128 + jnp.maximum(xs[d], 1) * PIECE, PIECE)
+        middle[d] = send.prepare(kv1.at[:, pl.ds(own, PIECE), :], kv1.at[:, pl.ds(to, PIECE), :], onward)
 
     def project_kv(g, d):
-        def one(i, _):
-            product = jnp.dot(rows_of(i, d), w_kv[g], preferred_element_type=F32).astype(BF16)
-            first = pl.multiple_of(HALO[g] + i * 128 + xs[d] * PIECE, PIECE)
-            kv[g][:, pl.ds(first, PIECE), :] = product.reshape(BATCH, PIECE, 2 * HEAD)
-            return 0
-
-        def run():
-            arrived(*token_needs[d])
-            lax.fori_loop(0, 2, one, 0)
-            if g == 2:
-                for core in (1, 0):
-                    first = core * 128 + xs[d] * PIECE
-                    start(
-                        f"w{core}.{d}",
-                        kv2.at[:, pl.ds(pl.multiple_of(384 + first, PIECE), PIECE), :],
-                        kv2.at[:, pl.ds(pl.multiple_of(128 + first, PIECE), PIECE), :],
-                        "h",
-                    )
+        def run():
+            need_tokens(d)
+            keep_kv(g, d, jnp.dot(rows_of(d), w_kv[g], preferred_element_type=F32))
+            if g == 1:
+                pl.when(xs[d] > 0)(middle[d].start)
+            else:
+                pl.when(xs[d] == 3)(near.start)
 
         return run
 
     def project_q(d):
-        def one(i, _):
-            product = jnp.dot(rows_of(i, d), w_q[...], preferred_element_type=F32).astype(BF16)
-            for g in range(3):
-                part = product[:, g * HEAD : (g + 1) * HEAD].reshape(BATCH, PIECE, HEAD)
-                queries[g, :, slab(i, xs[d]), :] = part
-            return 0
-
-        def run():
-            arrived(*token_needs[d])
-            lax.fori_loop(0, 2, one, 0)
-
-        return run
-
-    def forward_wide(d):
-        def run():
-            arrived(f"w1.{d}")
-            start(
-                f"f.{d}",
-                kv2.at[:, pl.ds(pl.multiple_of(256 + xs[d] * PIECE, PIECE), PIECE), :],
-                kv2.at[:, slab(0, xs[d]), :],
-                "h",
-            )
+        def run():
+            need_tokens(d)
+            product = jnp.dot(rows_of(d), w_q[...], preferred_element_type=F32)
+            product = product.astype(BF16).reshape(2, BATCH, PIECE, 3 * HEAD)
+            for core in range(2):
+                for g in range(3):
+                    queries[g, :, slab(core, xs[d]), :] = product[core, :, :, g * HEAD : (g + 1) * HEAD]
 
         return run
 
     for d in DELTAS:
-        for g in range(3):
-            setattr(parts[f"kv{g}"], f"project{d % 4}", project_kv(g, d))
+        for half in range(2):
+            setattr(kv2_part, f"project{d % 4}{half}", project_wide(d, half))
+            setattr(wide, f"onward{d % 4}{half}", forward_wide(d, half))
+        setattr(kv1_part, f"project{d % 4}", project_kv(1, d))
+        setattr(kv0_part, f"project{d % 4}", project_kv(0, d))
         setattr(q_part, f"project{d % 4}", project_q(d))
-        setattr(wide, f"onward{d % 4}", forward_wide(d))
-    kv1_part.halo = lambda: start("mid", kv1.at[:, pl.ds(ROWS, 96), :], kv1.at[:, pl.ds(0, 96), :], "h")
-    kv0_part.halo = lambda: start("near", kv0.at[:, pl.ds(ROWS, 32), :], kv0.at[:, pl.ds(0, 32), :], "h")
 
     def make_masks():
         own_logs[...] = jnp.zeros_like(own_logs)
@@ -382,29 +407,34 @@
 
     make_masks()
     order = (
-        tok.begin, kv2_part.begin, kv1_part.begin, kv2_part.up, kv2_part.down, kv2_part.up0,
+        kv2_part.begin, tok.begin, kv1_part.begin, kv2_part.up, kv2_part.down, kv2_part.up0,
         kv1_part.up, kv1_part.down, kv1_part.up0, kv2_part.far, kv2_part.up3, kv2_part.down1,
-        kv1_part.far, kv0_part.begin, wo_part.begin, kv1_part.up3, kv1_part.down1, kv2_part.down2,
-        tok.a, tok.b, kv0_part.one, wo_part.up, wo_part.down, kv1_part.down2,
-        kv0_part.next0, wo_part.up0, q_part.begin, kv0_part.two, wo_part.far, kv2_part.finish,
-        wo_part.up3, kv2_part.project0, kv0_part.next1, wo_part.down1, q_part.one, tok.c,
-        tok.d, kv0_part.back, kv1_part.finish, kv1_part.project0, kv0_part.last0, kv2_part.project3,
-        wide.onward0, q_part.next0, kv2_part.project1, q_part.two, kv0_part.next2, kv1_part.project1,
-        wo_part.down2, kv1_part.project3, kv0_part.last1, q_part.next1, q_part.back, kv0_part.next3,
-        wide.onward3, tok.e, tok.f, q_part.last0, q_part.next2, kv0_part.last2,
-        wo_part.finish, out.begin, kv2_part.project2, kv1_part.project2, kv1_part.halo, q_part.last1,
-        q_part.next3, kv0_part.last3, wide.onward1, q_part.last2, q_part.last3, kv0_part.finish,
-        kv0_part.project0, out.a, out.b, kv0_part.project1, kv0_part.project3, q_part.finish,
-        kv0_part.project2, kv0_part.halo, wide.onward2, q_part.project0, q_part.project1, q_part.project3,
-        out.c, out.d, q_part.project2, out.e,
+        kv1_part.far, wo_part.begin, kv1_part.up3, kv1_part.down1, kv2_part.down2, wo_part.one,
+        tok.a, tok.b, kv1_part.down2, wo_part.next0, kv0_part.begin, wo_part.two,
+        kv2_part.finish, kv2_part.project00, wo_part.next1, kv2_part.project01, kv2_part.project30, kv2_part.project11,
+        kv0_part.one, kv1_part.finish, kv1_part.project0, wo_part.back, wo_part.last0, kv0_part.next0,
+        q_part.begin, wide.onward00, wo_part.next2, wo_part.last1, kv0_part.two, kv0_part.next1,
+        wide.onward01, wo_part.next3, tok.c, tok.d, q_part.one, wide.onward30,
+        kv2_part.project31, kv0_part.last0, kv1_part.project3, kv0_part.back, kv2_part.project10, kv1_part.project1,
+        q_part.next0, wide.onward11, wo_part.last2, q_part.two, kv0_part.next2, kv0_part.last1,
+        wo_part.last3, tok.e, tok.f, q_part.next1, q_part.back, kv2_part.project20,
+        kv0_part.next3, wide.onward31, kv2_part.project21, q_part.last0, kv1_part.project2, q_part.next2,
+        kv0_part.last2, wide.onward10, wo_part.finish, out.begin, q_part.last1, q_part.next3,
+        kv0_part.last3, wide.onward20, q_part.last2, wide.onward21, out.a, out.b,
+        q_part.last3, kv0_part.finish, kv0_part.project0, kv0_part.project1, kv0_part.project3, kv0_part.project2,
+        q_part.finish, q_part.project0, q_part.project1, out.c, out.d, q_part.project3,
+        q_part.project2, out.e,
     )
     for step in order:
         step()
 
-    arrived(*(f"w{core}.{d}" for core in (1, 0) for d in DELTAS), "mid", "near")
+    arrived(*(f"w{core}{d}{half}" for core in (1, 0) for d in DELTAS for half in range(2)))
+    for d in DELTAS:
+        pl.when(xs[d] > 0)(middle[d].wait_recv)
+    near.wait_recv()
     attend(1)
     exchange(1)
-    arrived(*(f"f.{d}" for d in DELTAS))
+    arrived(*(f"f{d}{half}" for d in DELTAS for half in range(2)))
     attend(0)
     exchange(0)
     start("logs", own_logs.at[1 - c], partner_logs, "p")
@@ -436,8 +466,10 @@
         return 0
 
     lax.fori_loop(0, 4, out_tile, 0)
-    for copy in send.started + exchanged:
+    for copy in send.started + exchanged + [near]:
         copy.wait_send()
+    for d in DELTAS:
+        pl.when(xs[d] > 0)(middle[d].wait_send)
 
 
 def layer(tokens, norm_gain, w_query, w_key, w_value, w_out):

time: 91.1 us -> 84.1 us (0.923)
  Pallas kernels: 87.6 us -> 80.6 us
    pallas_call x1, Pallas kernels: 87.6 us -> 80.6 us  [layer(): pl.pallas_call(kernel, out_shape=(jax.ShapeDtypeStruct((BATCH, PIECE, WID...]
where the time goes in v3:
time: 84.1 us; the launch traced here: 83.9 us
  Pallas kernels  80.6 us (96%)
  local copies, waits for them, and re-layouts  2.69 us (3%)
    pallas_call x1, Pallas kernels, layer(): pl.pallas_call(kernel, out_shape=(jax.ShapeDtypeStruct((BATCH, PIECE, WID...  80.6 us
    unnamed x4, local copies, waits for them, and re-layouts  2.69 us

profile of v3, /device:TPU:0, one launch (start us, length us, event | category | flops | bytes accessed | tf_op | source)
XLA Modules:
  0.0 83.9 jit_solution(16926356264742298501)
XLA Ops:
  0.6 80.6 %shard_map.77 = (bf16[6,32,2048]{2,1,0:T(8,128)(2,1)}, f32[6,2,128]{2,1,0:T(2,128)}) custom-call(bf16[6,32,2048]{2,1,0:T(8,128)(2,1)} %bitcast.5, f32[1,2048]{1,0:T(1,128)} %bitcast.8, bf16[3,64,256]{2,1,0:T(8,128)(2,1)} %wq_ref.1, bf16[3,64,256]{2,1,0:T(8,128)(2,1)} %wk_ref.1, bf16[3,64,256]{2,1,0:T(8,128)(2,1)} %wv_ref.1, bf16[64,256]{1,0:T(8,128)(2,1)} %bitcast.7), custom_call_target="tpu_custom_call" | custom-call | tf_op jit(solution)/shard_map/pallas_call | solution.py:478
  81.2 0.0 copy-start
  81.2 2.1 %copy.10 = bf16[32,6,2048]{2,0,1:T(8,128)(2,1)} copy(bf16[32,6,2048]{2,0,1:T(8,128)(2,1)} %bitcast.6) | data formatting | bytes 1572864
  83.3 0.0 copy-done
  83.3 0.6 copy.11
Async XLA Ops:
  81.2 2.1 %copy-start = (f32[6,2,128]{2,1,0:T(2,128)S(1)}, f32[6,2,128]{2,1,0:T(2,128)}, u32[]{:S(2)}) copy-start(f32[6,2,128]{2,1,0:T(2,128)} %get-tuple-element.5) | copy-start | bytes 18436

commit v4 on v3

--- a/solution.py
+++ b/solution.py
@@ -19,12 +19,12 @@
 HALO = (32, 96, 384)
 SPAN = (160, 224, 512)
 DILATION = (1, 4, 16)
-COPIES = 200
-EXCHANGE = 192
+COPIES = 216
+EXCHANGE = 200
 F32 = jnp.float32
 BF16 = jnp.bfloat16
 DELTAS = (0, 1, -1, 2)
-LEAN = {"kv2": 0, "kv1": 0, "kv0": 2, "q": 2, "wo": 2}
+LEAN = {"kv2": 0, "kv1": 0, "kv0": 2, "q": 2, "wo": 0}
 NT = (((1,), (1,)), ((), ()))
 TN = (((0,), (0,)), ((), ()))
 
@@ -318,9 +318,16 @@
         middle[d] = send.prepare(kv1.at[:, pl.ds(own, PIECE), :], kv1.at[:, pl.ds(to, PIECE), :], onward)
 
     def project_kv(g, d):
+        def one(core, _):
+            rows = normed[:, slab(core, xs[d]), :].reshape(BATCH * PIECE, WIDTH)
+            product = jnp.dot(rows, w_kv[g], preferred_element_type=F32).astype(BF16)
+            first = pl.multiple_of(HALO[g] + core * 128 + xs[d] * PIECE, PIECE)
+            kv[g][:, pl.ds(first, PIECE), :] = product.reshape(BATCH, PIECE, 2 * HEAD)
+            return 0
+
         def run():
             need_tokens(d)
-            keep_kv(g, d, jnp.dot(rows_of(d), w_kv[g], preferred_element_type=F32))
+            lax.fori_loop(0, 2, one, 0)
             if g == 1:
                 pl.when(xs[d] > 0)(middle[d].start)
             else:
@@ -365,7 +372,7 @@
     scale = 1.0 / math.sqrt(HEAD)
     column_of_mine = pl.ds(pl.multiple_of((2 * x + c) * HEAD, HEAD), HEAD)
 
-    def attend(half):
+    def attend(half, part):
         def one(i, _):
             parts, row = [], 0
             for g in (2, 1, 0):
@@ -388,17 +395,18 @@
             heads[i, pl.ds(half * 128, 128), :] = (mixture / total).T.astype(BF16)
             return 0
 
-        lax.fori_loop(0, BATCH, one, 0, unroll=2)
+        lax.fori_loop(3 * part, 3 * part + 3, one, 0, unroll=3)
 
     exchanged = []
 
-    def exchange(half):
+    def exchange(half, part):
         for i, d in enumerate((2, 1, -1)):
+            slot = EXCHANGE + 6 * part + 2 * i
             copy = pltpu.make_async_remote_copy(
-                src_ref=heads.at[:, slab(half, xs[d]), :],
-                dst_ref=gathered.at[:, :, column_of_mine],
-                send_sem=send_sem.at[EXCHANGE + 2 * i + half],
-                recv_sem=recv_sem.at[EXCHANGE + 2 * i + c],
+                src_ref=heads.at[halves[part], slab(half, xs[d]), :],
+                dst_ref=gathered.at[halves[part], :, column_of_mine],
+                send_sem=send_sem.at[slot + half],
+                recv_sem=recv_sem.at[slot + c],
                 device_id=at(q, half, xs[d]),
                 device_id_type=MESH,
             )
@@ -407,23 +415,22 @@
 
     make_masks()
     order = (
-        kv2_part.begin, tok.begin, kv1_part.begin, kv2_part.up, kv2_part.down, kv2_part.up0,
-        kv1_part.up, kv1_part.down, kv1_part.up0, kv2_part.far, kv2_part.up3, kv2_part.down1,
-        kv1_part.far, wo_part.begin, kv1_part.up3, kv1_part.down1, kv2_part.down2, wo_part.one,
-        tok.a, tok.b, kv1_part.down2, wo_part.next0, kv0_part.begin, wo_part.two,
-        kv2_part.finish, kv2_part.project00, wo_part.next1, kv2_part.project01, kv2_part.project30, kv2_part.project11,
-        kv0_part.one, kv1_part.finish, kv1_part.project0, wo_part.back, wo_part.last0, kv0_part.next0,
-        q_part.begin, wide.onward00, wo_part.next2, wo_part.last1, kv0_part.two, kv0_part.next1,
-        wide.onward01, wo_part.next3, tok.c, tok.d, q_part.one, wide.onward30,
-        kv2_part.project31, kv0_part.last0, kv1_part.project3, kv0_part.back, kv2_part.project10, kv1_part.project1,
-        q_part.next0, wide.onward11, wo_part.last2, q_part.two, kv0_part.next2, kv0_part.last1,
-        wo_part.last3, tok.e, tok.f, q_part.next1, q_part.back, kv2_part.project20,
-        kv0_part.next3, wide.onward31, kv2_part.project21, q_part.last0, kv1_part.project2, q_part.next2,
-        kv0_part.last2, wide.onward10, wo_part.finish, out.begin, q_part.last1, q_part.next3,
-        kv0_part.last3, wide.onward20, q_part.last2, wide.onward21, out.a, out.b,
-        q_part.last3, kv0_part.finish, kv0_part.project0, kv0_part.project1, kv0_part.project3, kv0_part.project2,
-        q_part.finish, q_part.project0, q_part.project1, out.c, out.d, q_part.project3,
-        q_part.project2, out.e,
+        kv2_part.begin, tok.begin, kv1_part.begin, wo_part.begin, kv2_part.up, kv2_part.down,
+        kv2_part.up0, kv1_part.up, kv1_part.down, kv1_part.up0, wo_part.up, wo_part.down,
+        wo_part.up0, kv2_part.far, kv2_part.up3, kv1_part.far, kv2_part.down1, wo_part.far,
+        kv1_part.up3, kv1_part.down1, wo_part.down1, kv0_part.begin, kv2_part.down2, wo_part.up3,
+        tok.a, tok.b, kv1_part.down2, wo_part.down2, kv0_part.one, kv0_part.next0,
+        kv2_part.finish, kv2_part.project00, kv2_part.project01, kv2_part.project30, kv0_part.two, kv1_part.finish,
+        wo_part.finish, out.begin, kv1_part.project0, kv0_part.next1, kv2_part.project11, kv0_part.last0,
+        wide.onward00, tok.c, tok.d, kv0_part.back, q_part.begin, kv0_part.next2,
+        wide.onward01, kv0_part.last1, kv2_part.project31, kv1_part.project3, kv2_part.project10, kv1_part.project1,
+        wide.onward30, kv0_part.next3, q_part.one, q_part.next0, kv0_part.last2, wide.onward11,
+        tok.e, tok.f, kv0_part.last3, q_part.two, q_part.next1, kv2_part.project20,
+        kv2_part.project21, q_part.last0, kv1_part.project2, wide.onward31, q_part.back, kv0_part.finish,
+        kv0_part.project0, out.a, out.b, kv0_part.project1, q_part.next2, kv0_part.project3,
+        wide.onward10, q_part.last1, kv0_part.project2, q_part.next3, q_part.last2, out.c,
+        out.d, q_part.last3, wide.onward20, wide.onward21, q_part.finish, q_part.project0,
+        q_part.project1, out.e, q_part.project3, q_part.project2,
     )
     for step in order:
         step()
@@ -432,11 +439,13 @@
     for d in DELTAS:
         pl.when(xs[d] > 0)(middle[d].wait_recv)
     near.wait_recv()
-    attend(1)
-    exchange(1)
+    for part in range(2):
+        attend(1, part)
+        exchange(1, part)
     arrived(*(f"f{d}{half}" for d in DELTAS for half in range(2)))
-    attend(0)
-    exchange(0)
+    for part in range(2):
+        attend(0, part)
+        exchange(0, part)
     start("logs", own_logs.at[1 - c], partner_logs, "p")
     start("heads", heads.at[:, slab(1 - c, x), :], gathered.at[:, :, column_of_mine], "p")
     stay = local(heads.at[:, slab(c, x), :], gathered.at[:, :, column_of_mine], 11)
@@ -446,10 +455,10 @@
     logs_ref[:, 1, :] = jnp.where(c == 0, their_logs, mine_logs)[:BATCH]
     stay.wait()
     arrived("heads")
-    for slot in range(6):
+    for slot in range(12):
         pltpu.make_async_remote_copy(
-            src_ref=heads.at[:, pl.ds(0, PIECE), :],
-            dst_ref=gathered.at[:, :, column_of_mine],
+            src_ref=heads.at[halves[0], pl.ds(0, PIECE), :],
+            dst_ref=gathered.at[halves[slot // 6], :, column_of_mine],
             send_sem=send_sem.at[EXCHANGE + slot],
             recv_sem=recv_sem.at[EXCHANGE + slot],
             device_id=partner,

time: 84.1 us -> 80.2 us (0.954)
  Pallas kernels: 80.6 us -> 76.7 us
    pallas_call x1, Pallas kernels: 80.6 us -> 76.7 us  [layer(): pl.pallas_call(kernel, out_shape=(jax.ShapeDtypeStruct((BATCH, PIECE, WID...]
where the time goes in v4:
time: 80.2 us; the launch traced here: 80 us
  Pallas kernels  76.7 us (96%)
  local copies, waits for them, and re-layouts  2.69 us (3%)
    pallas_call x1, Pallas kernels, layer(): pl.pallas_call(kernel, out_shape=(jax.ShapeDtypeStruct((BATCH, PIECE, WID...  76.7 us
    unnamed x4, local copies, waits for them, and re-layouts  2.69 us

profile of v4, /device:TPU:0, one launch (start us, length us, event | category | flops | bytes accessed | tf_op | source)
XLA Modules:
  0.0 80.0 jit_solution(14689286457020994884)
XLA Ops:
  0.6 76.7 %shard_map.77 = (bf16[6,32,2048]{2,1,0:T(8,128)(2,1)}, f32[6,2,128]{2,1,0:T(2,128)}) custom-call(bf16[6,32,2048]{2,1,0:T(8,128)(2,1)} %bitcast.5, f32[1,2048]{1,0:T(1,128)} %bitcast.8, bf16[3,64,256]{2,1,0:T(8,128)(2,1)} %wq_ref.1, bf16[3,64,256]{2,1,0:T(8,128)(2,1)} %wk_ref.1, bf16[3,64,256]{2,1,0:T(8,128)(2,1)} %wv_ref.1, bf16[64,256]{1,0:T(8,128)(2,1)} %bitcast.7), custom_call_target="tpu_custom_call" | custom-call | tf_op jit(solution)/shard_map/pallas_call | solution.py:487
  77.3 0.0 copy-start
  77.3 2.1 %copy.10 = bf16[32,6,2048]{2,0,1:T(8,128)(2,1)} copy(bf16[32,6,2048]{2,0,1:T(8,128)(2,1)} %bitcast.6) | data formatting | bytes 1572864
  79.4 0.0 copy-done
  79.4 0.6 copy.11
Async XLA Ops:
  77.3 2.1 %copy-start = (f32[6,2,128]{2,1,0:T(2,128)S(1)}, f32[6,2,128]{2,1,0:T(2,128)}, u32[]{:S(2)}) copy-start(f32[6,2,128]{2,1,0:T(2,128)} %get-tuple-element.5) | copy-start | bytes 18436

commit v5 on v4

--- a/solution.py
+++ b/solution.py
@@ -474,7 +474,7 @@
         mixed_ref[:, :, columns] = product.astype(BF16).reshape(BATCH, PIECE, 512)
         return 0
 
-    lax.fori_loop(0, 4, out_tile, 0)
+    lax.fori_loop(0, 4, out_tile, 0, unroll=4)
     for copy in send.started + exchanged + [near]:
         copy.wait_send()
     for d in DELTAS:

time: 80.2 us -> 79.7 us (level)
  no operation moved by 1% of the time
where the time goes in v5:
time: 79.7 us; the launch traced here: 79.5 us
  Pallas kernels  76.2 us (96%)
  local copies, waits for them, and re-layouts  2.69 us (3%)
    pallas_call x1, Pallas kernels, layer(): pl.pallas_call(kernel, out_shape=(jax.ShapeDtypeStruct((BATCH, PIECE, WID...  76.2 us
    unnamed x4, local copies, waits for them, and re-layouts  2.69 us

profile of v5, /device:TPU:0, one launch (start us, length us, event | category | flops | bytes accessed | tf_op | source)
XLA Modules:
  0.0 79.5 jit_solution(2729356875710688030)
XLA Ops:
  0.6 76.2 %shard_map.77 = (bf16[6,32,2048]{2,1,0:T(8,128)(2,1)}, f32[6,2,128]{2,1,0:T(2,128)}) custom-call(bf16[6,32,2048]{2,1,0:T(8,128)(2,1)} %bitcast.5, f32[1,2048]{1,0:T(1,128)} %bitcast.8, bf16[3,64,256]{2,1,0:T(8,128)(2,1)} %wq_ref.1, bf16[3,64,256]{2,1,0:T(8,128)(2,1)} %wk_ref.1, bf16[3,64,256]{2,1,0:T(8,128)(2,1)} %wv_ref.1, bf16[64,256]{1,0:T(8,128)(2,1)} %bitcast.7), custom_call_target="tpu_custom_call" | custom-call | tf_op jit(solution)/shard_map/pallas_call | solution.py:487
  76.8 0.0 copy-start
  76.8 2.1 %copy.10 = bf16[32,6,2048]{2,0,1:T(8,128)(2,1)} copy(bf16[32,6,2048]{2,0,1:T(8,128)(2,1)} %bitcast.6) | data formatting | bytes 1572864
  78.9 0.0 copy-done
  78.9 0.6 copy.11
Async XLA Ops:
  76.8 2.1 %copy-start = (f32[6,2,128]{2,1,0:T(2,128)S(1)}, f32[6,2,128]{2,1,0:T(2,128)}, u32[]{:S(2)}) copy-start(f32[6,2,128]{2,1,0:T(2,128)} %get-tuple-element.5) | copy-start | bytes 18436

commit v6 on v5

--- a/solution.py
+++ b/solution.py
@@ -195,7 +195,7 @@
             normed[i, own_slab, :] = (scaled * gain_ref[...]).astype(BF16)
             return 0
 
-        lax.fori_loop(0, BATCH, one, 0)
+        lax.fori_loop(0, BATCH, one, 0, unroll=3)
         for half in range(2):
             pass_on(f"x+{half}", half, 0, "x+")
             pass_on(f"x-{1 - half}", 1 - half, 0, "x-")

time: 79.7 us -> 79.7 us (level)
  no operation moved by 1% of the time
where the time goes in v6:
time: 79.7 us; the launch traced here: 79.5 us
  Pallas kernels  76.2 us (96%)
  local copies, waits for them, and re-layouts  2.69 us (3%)
    pallas_call x1, Pallas kernels, layer(): pl.pallas_call(kernel, out_shape=(jax.ShapeDtypeStruct((BATCH, PIECE, WID...  76.2 us
    unnamed x4, local copies, waits for them, and re-layouts  2.69 us

profile of v6, /device:TPU:0, one launch (start us, length us, event | category | flops | bytes accessed | tf_op | source)
XLA Modules:
  0.0 79.5 jit_solution(5551523574725215407)
XLA Ops:
  0.6 76.2 %shard_map.77 = (bf16[6,32,2048]{2,1,0:T(8,128)(2,1)}, f32[6,2,128]{2,1,0:T(2,128)}) custom-call(bf16[6,32,2048]{2,1,0:T(8,128)(2,1)} %bitcast.5, f32[1,2048]{1,0:T(1,128)} %bitcast.8, bf16[3,64,256]{2,1,0:T(8,128)(2,1)} %wq_ref.1, bf16[3,64,256]{2,1,0:T(8,128)(2,1)} %wk_ref.1, bf16[3,64,256]{2,1,0:T(8,128)(2,1)} %wv_ref.1, bf16[64,256]{1,0:T(8,128)(2,1)} %bitcast.7), custom_call_target="tpu_custom_call" | custom-call | tf_op jit(solution)/shard_map/pallas_call | solution.py:487
  76.8 0.0 copy-start
  76.8 2.1 %copy.10 = bf16[32,6,2048]{2,0,1:T(8,128)(2,1)} copy(bf16[32,6,2048]{2,0,1:T(8,128)(2,1)} %bitcast.6) | data formatting | bytes 1572864
  78.9 0.0 copy-done
  78.9 0.6 copy.11
Async XLA Ops:
  76.8 2.1 %copy-start = (f32[6,2,128]{2,1,0:T(2,128)S(1)}, f32[6,2,128]{2,1,0:T(2,128)}, u32[]{:S(2)}) copy-start(f32[6,2,128]{2,1,0:T(2,128)} %get-tuple-element.5) | copy-start | bytes 18436
